TPU v7x, 256 devices: a whole 4x4x8 slice. The times are simulated.
256 devices in a mesh: sp: 16 (over y, x), tp: 16 (over z, core).
Axes of the slice: x: 4, y: 4, z: 8, core: 2. Of those that a mesh axis runs over, the one named last changes fastest.
Arguments:
- query_vectors: bfloat16 [16384, 16, 128], P('sp', 'tp'), may hold values from -6 to 6
- key_vectors: bfloat16 [16384, 16, 128], P('sp', 'tp'), may hold values from -6 to 6
- value_vectors: bfloat16 [16384, 16, 128], P('sp', 'tp'), may hold values from -6 to 6
- out_gate: bfloat16 [16384, 16, 128], P('sp', 'tp'), may hold values from -6 to 6
- decay_rate: float32 [2, 16], P(None, 'tp'), may hold values from 0 to 1
- decay_pre: float32 [2, 16, 16384], P(None, 'tp', 'sp'), may hold values from -6 to 6
- decay_shock: float32 [2, 16, 16384], P(None, 'tp', 'sp'), may hold values from -2 to 0
- beta_pre: float32 [2, 16, 16384], P(None, 'tp', 'sp'), may hold values from -12 to 0
- head_gain: float32 [128], replicated, may hold values from 0.1 to 1.9
- w_out: bfloat16 [2048, 2048], P('tp'), may hold values from -0.125 to 0.125
- tokens: bfloat16 [16384, 2048], P(('sp', 'tp')), may hold values from -6 to 6
- norm_gain: float32 [2048], replicated, may hold values from 0.1 to 1.9
- experts_pick: int32 [16384, 2], P(('sp', 'tp')), may hold values from 0 to 15, as said below
- pair_logits: float32 [16384, 2], P(('sp', 'tp')), may hold values from -6 to 6
- group_logits: float32 [16384, 8], P(('sp', 'tp')), may hold values from -6 to 6
- expert_gate: bfloat16 [16, 2048, 2048], P('sp', None, 'tp'), may hold values from -0.125 to 0.125
- expert_up: bfloat16 [16, 2048, 2048], P('sp', None, 'tp'), may hold values from -0.125 to 0.125
- expert_down: bfloat16 [16, 2048, 2048], P('sp', None, 'tp'), may hold values from -0.5 to 0.5
Outputs:
- layer_out: bfloat16 [16384, 2048], P(('sp', 'tp'))
Inputs may be any that keep to these rules, and one draw needn't show every extreme that they name: `experts_pick`: each token names two different experts of one group of 2 consecutive experts. The 64 tokens of one device fall 8 into each group. At most 8 tokens of one device name any one expert, and in every draw every expert is named by 8 tokens of every device.
All inputs are finite; a program needn't handle non-finite values.
Results may differ from a plain program's by a relative error of at most 0.02.
Values may be sent and summed in bfloat16 or wider, within the bound.
No kernel may reach another device: no remote copies, remote signals or barrier semaphores. Data moves between devices by JAX's collectives and lax.ppermute only.
A program may use at most 128 MiB of HBM per device.

v0:
```python
import jax
import jax.numpy as jnp
from jax import lax
from jax.sharding import Mesh
from jax.sharding import PartitionSpec as P

BLOCK = 64
GROUP_SIZE = 2
SP = ("sp_0", "sp_1")
SP_TP = ("sp_0", "sp_1", "tp")


NORM_EPSILON = 1e-06


def neutral_like(x, identity):
    return jax.tree.map(
        lambda part, zero: jnp.zeros_like(part) + jnp.asarray(zero, part.dtype), x, identity
    )


def prefix_by_axis(x, axes, combine, identity, reverse):
    before = start = neutral_like(x, identity)
    subtotal = x
    for axis in reversed(axes):
        peers, position = (lax.axis_size(axis), lax.axis_index(axis))
        pieces = jax.tree.map(
            lambda part, kind: lax.all_gather(part.astype(kind), axis),
            subtotal,
            (jnp.bfloat16, jnp.bfloat16),
        )
        inside, subtotal = (start, start)
        for k in reversed(range(peers)) if reverse else range(peers):
            passed = k > position if reverse else k < position
            subtotal = combine(
                subtotal, jax.tree.map(lambda part, own: part[k].astype(own.dtype), pieces, x)
            )
            inside = jax.tree.map(lambda new, old: jnp.where(passed, new, old), subtotal, inside)
        before = combine(inside, before)
    return before


def unit_rows(vectors):
    return vectors * lax.rsqrt(jnp.sum(vectors * vectors, axis=-1, keepdims=True) + NORM_EPSILON)


def block_sweep(queries, key_rows, value_rows, log_decay, beta_rate, start_state):
    length, value_width = value_rows.shape
    blocks = length // BLOCK
    query_blocks = queries.reshape(blocks, BLOCK, queries.shape[1])
    key_blocks = key_rows.reshape(blocks, BLOCK, key_rows.shape[1])
    value_blocks = value_rows.reshape(blocks, BLOCK, value_width)
    cumulative = jnp.cumsum(log_decay.reshape(blocks, BLOCK), axis=1)
    beta_blocks = beta_rate.reshape(blocks, BLOCK)
    position = jnp.arange(BLOCK)
    lower_mask = position[:, None] >= position[None, :]
    strict = position[:, None] > position[None, :]
    spread = cumulative[:, :, None] - cumulative[:, None, :]
    within = jnp.where(lower_mask, jnp.exp(jnp.where(lower_mask, spread, 0.0)), 0.0)
    scaled_keys = key_blocks * beta_blocks[:, :, None]
    lower_matrix = jnp.where(
        strict, jnp.einsum("nid,njd->nij", scaled_keys, key_blocks) * within, 0.0
    )
    identity = jnp.eye(BLOCK, dtype=jnp.float32)
    right_side = jnp.concatenate(
        [value_blocks * beta_blocks[:, :, None], scaled_keys * jnp.exp(cumulative)[:, :, None]],
        axis=2,
    )
    solved = jax.scipy.linalg.solve_triangular(
        lower_matrix + identity, right_side, lower=True, unit_diagonal=True
    )
    fresh_values = solved[:, :, :value_width]
    corrections = solved[:, :, value_width:]
    scores = jnp.einsum("nid,njd->nij", query_blocks, key_blocks) * within
    query_decayed = query_blocks * jnp.exp(cumulative)[:, :, None]
    block_total = cumulative[:, -1]
    decayed_keys = key_blocks * jnp.exp(block_total[:, None] - cumulative)[:, :, None]

    def advance(carried, inputs):
        values_in, fix_rows, query_in, key_in, score_in, total_in = inputs
        updated = values_in - jnp.dot(fix_rows, carried)
        output = jnp.dot(query_in, carried) + jnp.dot(score_in, updated)
        carried = carried * jnp.exp(total_in) + jnp.dot(key_in.T, updated)
        return (carried, output)

    final_state, outputs = lax.scan(
        advance,
        start_state,
        (fresh_values, corrections, query_decayed, decayed_keys, scores, block_total),
    )
    return (outputs.reshape(length, value_width), final_state)


def shards(
    query_vectors,
    key_vectors,
    value_vectors,
    out_gate,
    decay_rate,
    decay_pre,
    decay_shock,
    beta_pre,
    head_gain,
    w_out,
    tokens,
    norm_gain,
    experts_pick,
    pair_logits,
    group_logits,
    expert_gate,
    expert_up,
    expert_down,
):
    per_head_width = query_vectors.shape[2]
    queries = unit_rows(
        jnp.transpose(query_vectors.astype(jnp.float32), (1, 0, 2))
    ) * per_head_width ** (-0.5)
    keyset = unit_rows(jnp.transpose(key_vectors.astype(jnp.float32), (1, 0, 2)))
    valueset = jnp.transpose(value_vectors.astype(jnp.float32), (1, 0, 2))
    padded_values = jnp.concatenate([valueset, jnp.zeros_like(keyset)], axis=2)
    log_decay = jnp.moveaxis(
        -decay_rate[:, :, None] * jax.nn.softplus(decay_pre) + decay_shock, 1, 0
    )
    beta_rate = jnp.moveaxis(jax.nn.sigmoid(beta_pre), 1, 0)
    identity = jnp.eye(per_head_width, dtype=jnp.float32)
    opening = jnp.concatenate(
        [jnp.zeros((per_head_width, per_head_width), jnp.float32), identity], axis=1
    )

    def one_head(query_head, key_head, value_head, decay_head, beta_head):
        forward_result, ahead_end = block_sweep(
            query_head, key_head, value_head, decay_head[0], beta_head[0], opening
        )
        trailing_part, behind_end = block_sweep(
            query_head[::-1],
            key_head[::-1],
            value_head[::-1],
            decay_head[1, ::-1],
            beta_head[1, ::-1],
            opening,
        )
        return (forward_result, trailing_part[::-1], ahead_end, behind_end)

    forward_result, trailing_part, ahead_end, behind_end = jax.vmap(one_head)(
        queries, keyset, padded_values, log_decay, beta_rate
    )
    forward_shift = ahead_end[:, :, per_head_width:]
    forward_add = ahead_end[:, :, :per_head_width]
    backward_shift = behind_end[:, :, per_head_width:]
    backward_add = behind_end[:, :, :per_head_width]

    def compose(earlier, later):
        return (
            jnp.einsum("hij,hjk->hik", later[0], earlier[0]),
            jnp.einsum("hij,hjv->hiv", later[0], earlier[1]) + later[1],
        )

    neutral = (jnp.broadcast_to(identity, forward_shift.shape), jnp.zeros_like(forward_add))
    forward_carried = prefix_by_axis((forward_shift, forward_add), SP, compose, neutral, False)[1]
    backward_carried = prefix_by_axis((backward_shift, backward_add), SP, compose, neutral, True)[1]
    joined = (
        forward_result[:, :, :per_head_width]
        + trailing_part[:, :, :per_head_width]
        + jnp.einsum("qfc,qcj->qfj", forward_result[:, :, per_head_width:], forward_carried)
        + jnp.einsum("qfc,qcj->qfj", trailing_part[:, :, per_head_width:], backward_carried)
    )
    joined = jnp.transpose(joined, (1, 0, 2))
    head_scale = lax.rsqrt(jnp.mean(joined * joined, axis=-1, keepdims=True) + NORM_EPSILON)
    mixed_heads = (
        joined * head_scale * head_gain * jax.nn.silu(out_gate.astype(jnp.float32))
    ).astype(jnp.bfloat16)
    mixed_heads = mixed_heads.reshape(joined.shape[0], joined.shape[1] * per_head_width)
    local_rows = tokens.shape[0]
    part_sum = jnp.dot(mixed_heads, w_out, preferred_element_type=jnp.float32).astype(jnp.bfloat16)
    branch_sum = lax.psum_scatter(
        lax.optimization_barrier(part_sum).astype(jnp.float32).astype(jnp.bfloat16),
        "tp",
        scatter_dimension=0,
        tiled=True,
    ).astype(jnp.float32)
    residual = tokens.astype(jnp.float32) + branch_sum
    normed = (
        residual
        * lax.rsqrt(jnp.mean(residual * residual, axis=-1, keepdims=True) + NORM_EPSILON)
        * norm_gain
    ).astype(jnp.bfloat16)
    group_count = group_logits.shape[1]
    group_exp = jnp.exp(group_logits)
    group_share = group_exp / jnp.sum(group_exp, axis=-1, keepdims=True)
    group_index_of = experts_pick[:, 0] // GROUP_SIZE
    group_weight = jnp.sum(
        jnp.where(jnp.arange(group_count)[None, :] == group_index_of[:, None], group_share, 0.0),
        axis=1,
    )
    pair_exp = jnp.exp(pair_logits)
    route_weight = pair_exp / jnp.sum(pair_exp, axis=-1, keepdims=True) * group_weight[:, None]
    capacity = local_rows // group_count
    expert_count = lax.axis_size(SP)
    expert_marks = jnp.sum(
        (
            experts_pick[:, :, None] == jnp.arange(expert_count, dtype=jnp.int32)[None, None, :]
        ).astype(jnp.int32),
        axis=1,
    )
    earlier = jnp.cumsum(expert_marks, axis=0) - expert_marks
    slot_place = experts_pick * capacity + jnp.take_along_axis(earlier, experts_pick, axis=1)
    slot_index = jnp.arange(expert_count * capacity, dtype=jnp.int32)[:, None]
    chooser = (
        (slot_index == slot_place[None, :, 0]) | (slot_index == slot_place[None, :, 1])
    ).astype(jnp.bfloat16)
    outgoing = jnp.dot(chooser, normed, preferred_element_type=jnp.float32).astype(jnp.bfloat16)
    outgoing = outgoing.reshape(expert_count, capacity, normed.shape[1])
    arrived = lax.all_to_all(outgoing, SP, split_axis=0, concat_axis=0, tiled=True)
    source_count, slot_count, model_width = arrived.shape
    row_count = source_count * slot_count
    flat_rows = arrived.reshape(row_count, model_width)
    part_rows = lax.all_gather(flat_rows, "tp", axis=0, tiled=True)
    gate_out = jnp.dot(part_rows, expert_gate[0], preferred_element_type=jnp.float32)
    up_out = jnp.dot(part_rows, expert_up[0], preferred_element_type=jnp.float32)
    hidden = (jax.nn.silu(gate_out) * up_out).astype(jnp.bfloat16)
    product = lax.dot_general(
        hidden, expert_down[0], (((1,), (1,)), ((), ())), preferred_element_type=jnp.float32
    ).astype(jnp.bfloat16)
    summed_out = lax.psum_scatter(
        lax.optimization_barrier(product).astype(jnp.float32).astype(jnp.bfloat16),
        "tp",
        scatter_dimension=0,
        tiled=True,
    )
    expert_rows = summed_out.reshape(source_count, slot_count, model_width)
    results = lax.all_to_all(expert_rows, SP, split_axis=0, concat_axis=0, tiled=True)
    gathered = results.reshape(expert_count * capacity, normed.shape[1])
    chosen = gathered[slot_place]
    mixture = jnp.einsum("tk,tkd->td", route_weight, chosen.astype(jnp.float32))
    return (residual + mixture).astype(jnp.bfloat16)


def solution(mesh):
    finer = Mesh(mesh.devices.reshape(4, 4, mesh.shape["tp"]), ("sp_0", "sp_1", "tp"))
    in_specs = (
        P(SP, "tp", None),
        P(SP, "tp", None),
        P(SP, "tp", None),
        P(SP, "tp", None),
        P(None, "tp"),
        P(None, "tp", SP),
        P(None, "tp", SP),
        P(None, "tp", SP),
        P(),
        P("tp", None),
        P(SP_TP, None),
        P(),
        P(SP_TP, None),
        P(SP_TP, None),
        P(SP_TP, None),
        P(SP, None, "tp"),
        P(SP, None, "tp"),
        P(SP, None, "tp"),
    )
    out_specs = P(SP_TP, None)
    return jax.shard_map(
        shards, mesh=finer, in_specs=in_specs, out_specs=out_specs, check_vma=False
    )
```

profile of v0, /device:TPU:1, one launch (start us, length us, event | category | flops | bytes accessed | tf_op | source)
XLA Modules:
  0.0 672.9 jit_solution(16698587801744514501)
XLA Ops:
  6.5 1.2 fusion.92
  7.8 1.0 convert_element_type.213
  12.5 78.6 %custom-call.6 = f32[1,16,1,64,64]{3,4,2,1,0:T(8,128)S(1)} custom-call(f32[1,16,1,64,64]{4,3,2,1,0:T(8,128)S(1)} %fusion.59), custom_call_target="InvertDiagBlocksLowerTriangular" | custom-call | tf_op jit(solution)/shard_map/vmap(jit(_solve_triangular))/vmap()/triangular_solve | solution.py:69
  92.1 1.5 fusion.45
  93.6 1.1 slice_bitcast_fusion.1
  96.6 1.0 bitcast_multiply_fusion.2
  101.2 3.4 rev.17
  105.1 2.0 fusion.62
  107.1 79.4 %custom-call.7 = f32[1,16,1,64,64]{3,4,2,1,0:T(8,128)S(1)} custom-call(f32[1,16,1,64,64]{4,3,2,1,0:T(8,128)} %fusion.62), custom_call_target="InvertDiagBlocksLowerTriangular" | custom-call | tf_op jit(solution)/shard_map/vmap(jit(_solve_triangular))/vmap()/triangular_solve | solution.py:69
  187.1 1.5 fusion.44
  188.6 1.1 slice_bitcast_fusion
  192.6 53.2 %while.25 = (s32[]{:T(128)}, f32[1,128,256]{2,1,0:T(8,128)S(1)}, f32[16,1,64,256]{3,2,1,0:T(8,128)S(1)}, f32[16,1]{0,1:T(1,128)S(1)}, bf16[16,1,64,128]{3,2,1,0:...) while((s32[]{:T(128)}, f32[1,128,256]{2,1,0:T(8,128)S(1)}, ...), condition=%wide.region_7.9_spmd, body=%wide.region_6.8_spmd.sunk | while | flops 14794754 | bytes 952445 | solution.py:86
  195.9 1.0 convolution_subtract_fusion.5
  199.3 1.0 convolution_subtract_fusion.5
  202.6 1.0 convolution_subtract_fusion.5
  205.9 1.0 convolution_subtract_fusion.5
  209.2 1.0 convolution_subtract_fusion.5
  212.6 1.0 convolution_subtract_fusion.5
  215.9 1.0 convolution_subtract_fusion.5
  219.2 1.0 convolution_subtract_fusion.5
  222.6 1.0 convolution_subtract_fusion.5
  225.9 1.0 convolution_subtract_fusion.5
  229.2 1.0 convolution_subtract_fusion.5
  232.5 1.0 convolution_subtract_fusion.5
  235.9 1.0 convolution_subtract_fusion.5
  239.2 1.0 convolution_subtract_fusion.5
  242.5 1.0 convolution_subtract_fusion.5
  246.9 1.2 fusion.50
  248.9 54.2 %while.24 = (s32[]{:T(128)}, f32[1,128,256]{2,1,0:T(8,128)S(1)}, f32[16,1,64,256]{3,2,1,0:T(8,128)S(1)}, f32[16,1]{0,1:T(1,128)S(1)}, bf16[16,1,64,128]{3,2,1,0:...) while((s32[]{:T(128)}, f32[1,128,256]{2,1,0:T(8,128)S(1)}, ...), condition=%wide.region_4.6_spmd, body=%wide.region_3.5_spmd.sunk | while | flops 14794754 | bytes 952445 | solution.py:86
  248.9 1.0 convolution_subtract_fusion.4
  252.3 1.0 convolution_subtract_fusion.4
  255.7 1.0 convolution_subtract_fusion.4
  259.1 1.0 convolution_subtract_fusion.4
  265.8 1.0 convolution_subtract_fusion.4
  269.2 1.0 convolution_subtract_fusion.4
  272.6 1.0 convolution_subtract_fusion.4
  292.9 1.0 convolution_subtract_fusion.4
  303.1 10.3 %all-gather = bf16[4,128,128]{2,1,0:T(8,128)(2,1)S(1)} all-gather(bf16[1,128,128]{2,1,0:T(8,128)(2,1)S(1)} %get-tuple-element.234), channel_id=2, replica_groups=mesh['sp_0'=4,'sp_1'=4,'tp'=16] {'sp_1'}, dimensions={0}, use_global_device_ids=true | all-gather | bytes 163840 | tf_op jit(solution)/shard_map/all_gather | solution.py:28
  314.6 9.6 %all-gather.1 = bf16[512,128]{1,0:T(8,128)(2,1)S(1)} all-gather(bf16[128,128]{1,0:T(8,128)(2,1)S(1)} %fusion.226), channel_id=3, replica_groups=mesh['sp_0'=4,'sp_1'=4,'tp'=16] {'sp_0'}, dimensions={0}, use_global_device_ids=true | all-gather | bytes 163840 | tf_op jit(solution)/shard_map/all_gather | solution.py:28
  324.2 9.3 %all-gather.2 = bf16[4,128,128]{2,1,0:T(8,128)(2,1)S(1)} all-gather(bf16[1,128,128]{2,1,0:T(8,128)(2,1)S(1)} %get-tuple-element.235), channel_id=4, replica_groups=mesh['sp_0'=4,'sp_1'=4,'tp'=16] {'sp_1'}, dimensions={0}, use_global_device_ids=true | all-gather | bytes 163840 | tf_op jit(solution)/shard_map/all_gather | solution.py:28
  334.6 9.1 %all-gather.3 = bf16[512,128]{1,0:T(8,128)(2,1)S(1)} all-gather(bf16[128,128]{1,0:T(8,128)(2,1)S(1)} %convolution_add_fusion.15), channel_id=5, replica_groups=mesh['sp_0'=4,'sp_1'=4,'tp'=16] {'sp_0'}, dimensions={0}, use_global_device_ids=true | all-gather | bytes 163840 | tf_op jit(solution)/shard_map/all_gather | solution.py:28
  344.8 9.1 %all-gather.4 = bf16[4,128,128]{2,1,0:T(8,128)(2,1)S(1)} all-gather(bf16[1,128,128]{2,1,0:T(8,128)(2,1)S(1)} %get-tuple-element.236), channel_id=6, replica_groups=mesh['sp_0'=4,'sp_1'=4,'tp'=16] {'sp_1'}, dimensions={0}, use_global_device_ids=true | all-gather | bytes 163840 | tf_op jit(solution)/shard_map/all_gather | solution.py:28
  355.5 9.6 %all-gather.5 = bf16[512,128]{1,0:T(8,128)(2,1)S(1)} all-gather(bf16[128,128]{1,0:T(8,128)(2,1)S(1)} %fusion.229), channel_id=7, replica_groups=mesh['sp_0'=4,'sp_1'=4,'tp'=16] {'sp_0'}, dimensions={0}, use_global_device_ids=true | all-gather | bytes 163840 | tf_op jit(solution)/shard_map/all_gather | solution.py:28
  365.1 9.1 %all-gather.6 = bf16[4,128,128]{2,1,0:T(8,128)(2,1)S(1)} all-gather(bf16[1,128,128]{2,1,0:T(8,128)(2,1)S(1)} %get-tuple-element.237), channel_id=8, replica_groups=mesh['sp_0'=4,'sp_1'=4,'tp'=16] {'sp_1'}, dimensions={0}, use_global_device_ids=true | all-gather | bytes 163840 | tf_op jit(solution)/shard_map/all_gather | solution.py:28
  375.8 9.1 %all-gather.7 = bf16[512,128]{1,0:T(8,128)(2,1)S(1)} all-gather(bf16[128,128]{1,0:T(8,128)(2,1)S(1)} %convolution_add_fusion.6), channel_id=9, replica_groups=mesh['sp_0'=4,'sp_1'=4,'tp'=16] {'sp_0'}, dimensions={0}, use_global_device_ids=true | all-gather | bytes 163840 | tf_op jit(solution)/shard_map/all_gather | solution.py:28
  387.5 1.0 copy.130
  388.6 3.9 slice.185
  392.5 1.2 fusion.64
  393.7 2.0 convolution_bitcast_fusion.2
  395.8 1.7 fusion.68
  397.5 1.5 multiply_reduce_fusion.1
  399.0 1.1 copy.119
  400.1 4.3 convolution_convert_fusion.1
  405.6 1.3 gather_fusion.1
  407.2 81.1 %reduce-scatter.3.cloned.1.call-done = bf16[64,2048]{1,0:T(8,128)(2,1)} async-done(((bf16[1024,2048]{1,0:T(8,128)(2,1)}), bf16[64,2048]{1,0:T(8,128)(2,1)}) %reduce-scatter.3.cloned.1.call-update) | async-done | bytes 262160 | tf_op jit(solution)/shard_map/reduce_scatter | solution.py:175
  488.3 1.1 multiply_reduce_fusion
  489.5 1.3 fusion.37
  490.8 15.3 %all_to_all.10 = bf16[16,8,2048]{2,1,0:T(8,128)(2,1)} all-to-all(bf16[16,8,2048]{2,1,0:T(8,128)(2,1)S(1)} %fusion.37), channel_id=1, replica_groups=mesh['sp_0'=4,'sp_1'=4,'tp'=16] {'sp_0','sp_1'}, dimensions={0} | all-to-all | bytes 1048576 | tf_op jit(solution)/shard_map/all_to_all | solution.py:213
  506.2 56.6 %all-gather.10.cloned.1.call-done = bf16[2048,2048]{1,0:T(8,128)(2,1)} async-done(((bf16[128,2048]{1,0:T(8,128)(2,1)}), bf16[2048,2048]{1,0:T(8,128)(2,1)}) %all-gather.10.cloned.1.call-update) | async-done | bytes 8388624 | tf_op jit(solution)/shard_map/all_gather | solution.py:217
  562.8 5.7 fusion.86
  568.6 12.8 %convolution_convert_fusion = bf16[2048,2048]{1,0:T(8,128)(2,1)} fusion(bf16[2048,2048]{1,0:T(8,128)(2,1)} %all-gather.10.cloned.1.call-done, f32[2048,128]{1,0:T(8,128)S(1)} %fusion.86, bf16[1,2048,128]{2,1,0:T(8,128)(2,1)S(1)} %copy-done, bf16[1,2048,128]{2,1,0:T(8,128)(2,1)S(1)} %copy-done.6), kind=kOutput, calls=%fused_computation.46 | convolution fusion | flops 2153250816 | bytes 18874368 | tf_op jit(solution)/shard_map/dot_general | solution.py:221
  582.1 65.4 %reduce-scatter.5.cloned.1.call-done = bf16[128,2048]{1,0:T(8,128)(2,1)} async-done(((bf16[2048,2048]{1,0:T(8,128)(2,1)}), bf16[128,2048]{1,0:T(8,128)(2,1)}) %reduce-scatter.5.cloned.1.call-update) | async-done | bytes 524304 | tf_op jit(solution)/shard_map/reduce_scatter | solution.py:224
  647.6 6.5 all-to-all-start.1
  654.6 8.9 %all-to-all-done.1 = bf16[16,8,2048]{2,1,0:T(8,128)(2,1)S(1)} async-done(((bf16[16,8,2048]{2,1,0:T(8,128)(2,1)}), bf16[16,8,2048]{2,1,0:T(8,128)(2,1)S(1)}, u32[]{:S(2)}, u32[]{:S(2)}) %all-to-all-start.1) | async-done | bytes 524320 | tf_op jit(solution)/shard_map/all_to_all | solution.py:231
  (365 shorter events, 114.0 us)
Async XLA Ops:
  6.5 562.0 %copy-start = (bf16[1,2048,128]{2,1,0:T(8,128)(2,1)S(1)}, bf16[1,2048,128]{2,1,0:T(8,128)(2,1)}, u32[]{:S(2)}) copy-start(bf16[1,2048,128]{2,1,0:T(8,128)(2,1)} %param.41) | copy-start | bytes 1572868
  6.5 481.8 %reduce-scatter.3.cloned.1.call-start = ((), (), s32[]{:S(2)}) async-start(), calls=%async_computation.4 | async-start | bytes 4456448 | tf_op jit(solution)/shard_map/reduce_scatter | solution.py:175
  7.8 83.5 %copy-start.22 = (bf16[1024,1,128]{2,0,1:T(8,128)(2,1)S(1)}, bf16[1024,1,128]{2,0,1:T(8,128)(2,1)}, u32[]{:S(2)}) copy-start(bf16[1024,1,128]{2,0,1:T(8,128)(2,1)} %param.26) | copy-start | bytes 786436
  8.8 82.5 %copy-start.41 = (f32[64,64]{1,0:T(8,128)}, f32[64,64]{1,0:T(8,128)S(1)}, u32[]{:S(2)}) copy-start(f32[64,64]{1,0:T(8,128)S(1)} %get-tuple-element.256) | copy-start | bytes 49156
  8.8 82.5 %copy-start.47 = (pred[64,64]{1,0:T(8,128)(4,1)}, pred[64,64]{1,0:T(8,128)(4,1)S(1)}, u32[]{:S(2)}) copy-start(pred[64,64]{1,0:T(8,128)(4,1)S(1)} %get-tuple-element.255) | copy-start | bytes 12292
  8.9 82.5 %copy-start.42 = (f32[64,64]{1,0:T(8,128)}, f32[64,64]{1,0:T(8,128)S(1)}, u32[]{:S(2)}) copy-start(f32[64,64]{1,0:T(8,128)S(1)} %fusion.185) | copy-start | bytes 49156
  11.3 80.0 %copy-start.49 = (pred[64,64]{1,0:T(8,128)(4,1)}, pred[64,64]{1,0:T(8,128)(4,1)S(1)}, u32[]{:S(2)}) copy-start(pred[64,64]{1,0:T(8,128)(4,1)S(1)} %get-tuple-element.253) | copy-start | bytes 12292
  11.8 79.6 %copy-start.51 = (f32[16]{0:T(128)}, f32[16]{0:T(128)S(1)}, u32[]{:S(2)}) copy-start(f32[16]{0:T(128)S(1)} %slice_reduce_fusion.1) | copy-start | bytes 196
  93.6 1.9 copy-start.4
  93.6 2.9 copy-start.3
  97.6 7.5 %copy-start.48 = (pred[64,64]{1,0:T(8,128)(4,1)S(1)}, pred[64,64]{1,0:T(8,128)(4,1)}, u32[]{:S(2)}) copy-start(pred[64,64]{1,0:T(8,128)(4,1)} %copy-done.47) | copy-start | bytes 12292
  105.1 81.7 %copy-start.53 = (f32[16]{0:T(128)}, f32[16]{0:T(128)S(1)}, u32[]{:S(2)}) copy-start(f32[16]{0:T(128)S(1)} %slice_reduce_fusion) | copy-start | bytes 196
  192.0 0.6 copy-start.54
  245.8 1.0 copy-start.5
  248.1 0.8 copy-start.52
  313.5 0.6 copy-start.32
  314.3 9.9 %copy-start.23 = (bf16[128,128]{1,0:T(8,128)(2,1)}, bf16[128,128]{1,0:T(8,128)(2,1)S(1)}, u32[]{:S(2)}) copy-start(bf16[128,128]{1,0:T(8,128)(2,1)S(1)} %fusion.228) | copy-start | bytes 98308
  314.4 9.8 %copy-start.25 = (bf16[128,128]{1,0:T(8,128)(2,1)}, bf16[128,128]{1,0:T(8,128)(2,1)S(1)}, u32[]{:S(2)}) copy-start(bf16[128,128]{1,0:T(8,128)(2,1)S(1)} %fusion.227) | copy-start | bytes 98308
  314.5 9.6 %copy-start.27 = (bf16[128,128]{1,0:T(8,128)(2,1)}, bf16[128,128]{1,0:T(8,128)(2,1)S(1)}, u32[]{:S(2)}) copy-start(bf16[128,128]{1,0:T(8,128)(2,1)S(1)} %fusion.226) | copy-start | bytes 98308
  333.6 21.3 %copy-start.10 = (bf16[128,128]{1,0:T(8,128)(2,1)}, bf16[128,128]{1,0:T(8,128)(2,1)S(1)}, u32[]{:S(2)}) copy-start(bf16[128,128]{1,0:T(8,128)(2,1)S(1)} %convolution_add_fusion.18) | copy-start | bytes 98308
  333.7 0.6 copy-start.14
  334.5 20.5 %copy-start.16 = (bf16[128,128]{1,0:T(8,128)(2,1)}, bf16[128,128]{1,0:T(8,128)(2,1)S(1)}, u32[]{:S(2)}) copy-start(bf16[128,128]{1,0:T(8,128)(2,1)S(1)} %convolution_add_fusion.16) | copy-start | bytes 98308
  334.6 20.3 %copy-start.12 = (bf16[128,128]{1,0:T(8,128)(2,1)}, bf16[128,128]{1,0:T(8,128)(2,1)S(1)}, u32[]{:S(2)}) copy-start(bf16[128,128]{1,0:T(8,128)(2,1)S(1)} %convolution_add_fusion.15) | copy-start | bytes 98308
  343.7 41.5 %copy-start.7 = (bf16[512,128]{1,0:T(8,128)(2,1)}, bf16[512,128]{1,0:T(8,128)(2,1)S(1)}, u32[]{:S(2)}) copy-start(bf16[512,128]{1,0:T(8,128)(2,1)S(1)} %all-gather.3) | copy-start | bytes 393220
  343.9 0.9 copy-start.35
  344.0 0.8 copy-start.38
  354.0 0.6 copy-start.34
  354.8 0.6 copy-start.29
  355.4 9.7 %copy-start.30 = (bf16[128,128]{1,0:T(8,128)(2,1)}, bf16[128,128]{1,0:T(8,128)(2,1)S(1)}, u32[]{:S(2)}) copy-start(bf16[128,128]{1,0:T(8,128)(2,1)S(1)} %fusion.230) | copy-start | bytes 98308
  355.5 18.7 %copy-start.31 = (bf16[128,128]{1,0:T(8,128)(2,1)}, bf16[128,128]{1,0:T(8,128)(2,1)S(1)}, u32[]{:S(2)}) copy-start(bf16[128,128]{1,0:T(8,128)(2,1)S(1)} %fusion.229) | copy-start | bytes 98308
  365.1 22.2 %copy-start.8 = (bf16[512,128]{1,0:T(8,128)(2,1)}, bf16[512,128]{1,0:T(8,128)(2,1)S(1)}, u32[]{:S(2)}) copy-start(bf16[512,128]{1,0:T(8,128)(2,1)S(1)} %all-gather.5) | copy-start | bytes 393220
  374.3 0.6 copy-start.18
  374.5 0.6 copy-start.20
  375.1 0.6 copy-start.21
  375.8 9.4 %copy-start.19 = (bf16[128,128]{1,0:T(8,128)(2,1)}, bf16[128,128]{1,0:T(8,128)(2,1)S(1)}, u32[]{:S(2)}) copy-start(bf16[128,128]{1,0:T(8,128)(2,1)S(1)} %convolution_add_fusion.6) | copy-start | bytes 98308
  384.9 2.3 copy-start.9
  385.1 0.6 copy-start.37
  385.7 0.6 copy-start.40
  388.6 7.2 %copy-start.24 = (bf16[128,128]{1,0:T(8,128)(2,1)S(1)}, bf16[128,128]{1,0:T(8,128)(2,1)}, u32[]{:S(2)}) copy-start(bf16[128,128]{1,0:T(8,128)(2,1)} %copy-done.23) | copy-start | bytes 98308
  388.6 7.2 %copy-start.26 = (bf16[128,128]{1,0:T(8,128)(2,1)S(1)}, bf16[128,128]{1,0:T(8,128)(2,1)}, u32[]{:S(2)}) copy-start(bf16[128,128]{1,0:T(8,128)(2,1)} %copy-done.25) | copy-start | bytes 98308
  388.6 7.2 %copy-start.28 = (bf16[128,128]{1,0:T(8,128)(2,1)S(1)}, bf16[128,128]{1,0:T(8,128)(2,1)}, u32[]{:S(2)}) copy-start(bf16[128,128]{1,0:T(8,128)(2,1)} %copy-done.27) | copy-start | bytes 98308
  388.6 7.2 %copy-start.33 = (bf16[128,128]{1,0:T(8,128)(2,1)S(1)}, bf16[128,128]{1,0:T(8,128)(2,1)}, u32[]{:S(2)}) copy-start(bf16[128,128]{1,0:T(8,128)(2,1)} %copy-done.32) | copy-start | bytes 98308
  388.6 7.2 %copy-start.36 = (bf16[128,128]{1,0:T(8,128)(2,1)S(1)}, bf16[128,128]{1,0:T(8,128)(2,1)}, u32[]{:S(2)}) copy-start(bf16[128,128]{1,0:T(8,128)(2,1)} %copy-done.35) | copy-start | bytes 98308
  388.6 7.2 %copy-start.39 = (bf16[128,128]{1,0:T(8,128)(2,1)S(1)}, bf16[128,128]{1,0:T(8,128)(2,1)}, u32[]{:S(2)}) copy-start(bf16[128,128]{1,0:T(8,128)(2,1)} %copy-done.38) | copy-start | bytes 98308
  388.6 7.2 %copy-start.43 = (bf16[128,128]{1,0:T(8,128)(2,1)S(1)}, bf16[128,128]{1,0:T(8,128)(2,1)}, u32[]{:S(2)}) copy-start(bf16[128,128]{1,0:T(8,128)(2,1)} %convolution_add_fusion.13) | copy-start | bytes 98308
  388.6 8.9 %copy-start.11 = (bf16[128,128]{1,0:T(8,128)(2,1)S(1)}, bf16[128,128]{1,0:T(8,128)(2,1)}, u32[]{:S(2)}) copy-start(bf16[128,128]{1,0:T(8,128)(2,1)} %copy-done.10) | copy-start | bytes 98308
  388.6 8.9 %copy-start.13 = (bf16[128,128]{1,0:T(8,128)(2,1)S(1)}, bf16[128,128]{1,0:T(8,128)(2,1)}, u32[]{:S(2)}) copy-start(bf16[128,128]{1,0:T(8,128)(2,1)} %copy-done.12) | copy-start | bytes 98308
  388.6 8.8 %copy-start.15 = (bf16[128,128]{1,0:T(8,128)(2,1)S(1)}, bf16[128,128]{1,0:T(8,128)(2,1)}, u32[]{:S(2)}) copy-start(bf16[128,128]{1,0:T(8,128)(2,1)} %copy-done.14) | copy-start | bytes 98308
  388.6 8.8 %copy-start.17 = (bf16[128,128]{1,0:T(8,128)(2,1)S(1)}, bf16[128,128]{1,0:T(8,128)(2,1)}, u32[]{:S(2)}) copy-start(bf16[128,128]{1,0:T(8,128)(2,1)} %copy-done.16) | copy-start | bytes 98308
  397.5 2.6 copy-start.50
  404.5 0.7 copy-start.45
  404.5 158.3 %all-gather.10.cloned.1.call-start = ((), (), s32[]{:S(2)}) async-start(), calls=%async_computation.5 | async-start | bytes 8912896 | tf_op jit(solution)/shard_map/all_gather | solution.py:217
  405.6 82.7 %copy-start.1 = (bf16[64,2048]{1,0:T(8,128)(2,1)S(1)}, bf16[64,2048]{1,0:T(8,128)(2,1)}, u32[]{:S(2)}) copy-start(bf16[64,2048]{1,0:T(8,128)(2,1)} %param.34) | copy-start | bytes 786436
  405.6 83.8 %copy-start.46 = (f32[2048]{0:T(1024)S(1)}, f32[2048]{0:T(1024)}, u32[]{:S(2)}) copy-start(f32[2048]{0:T(1024)} %param.35) | copy-start | bytes 24580
  407.1 155.7 %copy-start.56 = (bf16[1,2048,128]{2,1,0:T(8,128)(2,1)S(1)}, bf16[1,2048,128]{2,1,0:T(8,128)(2,1)}, u32[]{:S(2)}) copy-start(bf16[1,2048,128]{2,1,0:T(8,128)(2,1)} %param.39) | copy-start | bytes 1572868
  506.1 62.4 %copy-start.6 = (bf16[1,2048,128]{2,1,0:T(8,128)(2,1)S(1)}, bf16[1,2048,128]{2,1,0:T(8,128)(2,1)}, u32[]{:S(2)}) copy-start(bf16[1,2048,128]{2,1,0:T(8,128)(2,1)} %param.40) | copy-start | bytes 1572868
  506.2 141.4 %reduce-scatter.5.cloned.1.call-start = ((), (), s32[]{:S(2)}) async-start(), calls=%async_computation.6 | async-start | bytes 8912896 | tf_op jit(solution)/shard_map/reduce_scatter | solution.py:224
  581.4 0.7 copy-start.44
  581.4 72.7 %copy-start.55 = (f32[64,2]{0,1:T(2,128)S(1)}, f32[64,2]{0,1:T(2,128)}, u32[]{:S(2)}) copy-start(f32[64,2]{0,1:T(2,128)} %param.37) | copy-start | bytes 1540
  647.6 15.8 %all-to-all-start.1 = ((bf16[16,8,2048]{2,1,0:T(8,128)(2,1)}), bf16[16,8,2048]{2,1,0:T(8,128)(2,1)S(1)}, u32[]{:S(2)}, u32[]{:S(2)}) async-start(bf16[16,8,2048]{2,1,0:T(8,128)(2,1)} %bitcast.435), calls=%async_computation.3 | async-start | bytes 1048576 | tf_op jit(solution)/shard_map/all_to_all | solution.py:231
  664.4 1.0 copy-start.2
Sparse Core Ops, SparseCore 0:
  404.6 83.6 reduce-scatter.2
  506.3 56.5 all-gather.9
  581.6 65.9 reduce-scatter.4
where the time goes:
time: 682 us; the launch traced here: 673 us
  waiting for transfers between devices  212 us (31%)
  other arithmetic  171 us (25%)
  matrix products  132 us (19%)
  blocking collectives  90.5 us (13%)
  local copies, waits for them, and re-layouts  46 us (7%)
  between operations  14.1 us (2%)
    another operation x5, other arithmetic, block_sweep(): jax.scipy.linalg.solve_triangular(lower_matrix + identity, right_side, lo...  158 us
    reduce_scatter x1, waiting for transfers between devices, shards(): lax.psum_scatter(lax.optimization_barrier(part_sum).astype(jnp.float32).a...  81.1 us
    all_gather x8, blocking collectives, prefix_by_axis(): lax.all_gather(part.astype(kind), axis)  75.2 us
    reduce_scatter x1, waiting for transfers between devices, shards(): lax.psum_scatter(lax.optimization_barrier(product).astype(jnp.float32).as...  65.4 us
    all_gather x1, waiting for transfers between devices, shards(): part_rows = lax.all_gather(flat_rows, 'tp', axis=0, tiled=True)  56.6 us
    dot_general x32, matrix products, advance(): updated = values_in - jnp.dot(fix_rows, carried)  31.8 us
    dot_general x64, matrix products, advance(): output = jnp.dot(query_in, carried) + jnp.dot(score_in, updated)  31.7 us
    dot_general x32, matrix products, advance(): carried = carried * jnp.exp(total_in) + jnp.dot(key_in.T, updated)  24.8 us
  transfers between devices with their start and end apart: 4, of which 4 were waited for; matrix products, arithmetic and copies ran while one was open for 0% of the time, Pallas kernels for 0%

commit v1 on v0

v1 whole, which is shorter than its diff:
```python
import jax
import jax.numpy as jnp
from jax import lax
from jax.experimental import pallas as pl
from jax.experimental.pallas import tpu as pltpu
from jax.sharding import Mesh
from jax.sharding import PartitionSpec as P

CHUNK = 128
GROUP_SIZE = 2
EPS = 1e-06
SP = ("sp_0", "sp_1")
SP_TP = ("sp_0", "sp_1", "tp")
F32 = jnp.float32
BF16 = jnp.bfloat16
PAIRED = 2


def mm(a, b):
    return jnp.dot(a, b, preferred_element_type=F32)


def mm_nt(a, b):
    return lax.dot_general(a, b, (((1,), (1,)), ((), ())), preferred_element_type=F32)


def iota2(shape, dim):
    return lax.broadcasted_iota(jnp.int32, shape, dim)


def local_kernel(rate_ref, q_ref, k_ref, v_ref, pre_ref, shock_ref, bpre_ref,
                 out_ref, reach_ref, maps_ref,
                 mask_ref, row_ref, col_ref, qeff_ref, add_ref, cut_ref):
    C = CHUNK
    length = q_ref.shape[0]
    chunks = length // C
    dh = q_ref.shape[1]
    scale = dh ** -0.5
    row = iota2((C, C), 0)
    col = iota2((C, C), 1)
    spans = []
    span = 1
    while span < C:
        spans.append(span)
        span *= 2
    for level, span in enumerate(spans):
        same = (row // (2 * span)) == (col // (2 * span))
        lower = same & ((row // span) % 2 == 1) & ((col // span) % 2 == 0)
        upper = same & ((row // span) % 2 == 0) & ((col // span) % 2 == 1)
        mask_ref[0, level] = lower.astype(F32).astype(BF16)
        mask_ref[1, level] = upper.astype(F32).astype(BF16)

    rows = 2 * chunks
    first = iota2((rows, C), 0) < chunks
    rate = jnp.where(first, rate_ref[0, 0], rate_ref[1, 0])
    pre = pre_ref[...]
    soft = jnp.maximum(pre, 0.0) + jnp.log1p(jnp.exp(-jnp.abs(pre)))
    decay = -rate * soft + shock_ref[...]
    beta = 1.0 / (1.0 + jnp.exp(-bpre_ref[...]))
    tri = (row <= col).astype(F32)
    tri_back = (row >= col).astype(F32)
    ahead = jnp.dot(decay, tri, precision=lax.Precision.HIGHEST, preferred_element_type=F32)
    behind = jnp.dot(decay, tri_back, precision=lax.Precision.HIGHEST, preferred_element_type=F32)
    summed = jnp.where(first, ahead, behind)
    total = jnp.where(first[:, :1], summed[:, C - 1:], summed[:, :1])
    row_ref[0] = summed
    row_ref[1] = beta
    row_ref[2] = beta * jnp.exp(summed)
    row_ref[3] = jnp.broadcast_to(jnp.exp(total), (rows, C))
    stacked = jnp.concatenate([summed, beta, jnp.exp(summed), jnp.exp(total - summed)], axis=0)
    stacked = jnp.concatenate([stacked, jnp.zeros((C - 4 * rows, C), F32)], axis=0) if 4 * rows < C else stacked
    turned = stacked.T
    for part in range(4):
        for r in range(rows):
            if part == 0:
                col_ref[part, r] = jnp.broadcast_to(turned[:, r:r + 1], (C, C))
            else:
                col_ref[part, r] = jnp.broadcast_to(turned[:, part * rows + r:part * rows + r + 1], (C, C))

    eye = (row == col).astype(F32)

    def body(step, carry):
        work = []
        for u in range(PAIRED):
            n = step * PAIRED + u
            here = pl.ds(pl.multiple_of(n * C, C), C)
            q = q_ref[here, :].astype(F32)
            k = k_ref[here, :].astype(F32)
            v = v_ref[here, :]
            qn = q * lax.rsqrt(jnp.sum(q * q, axis=1, keepdims=True) + EPS) * scale
            kn = k * lax.rsqrt(jnp.sum(k * k, axis=1, keepdims=True) + EPS)
            kb = kn.astype(BF16)
            qb = qn.astype(BF16)
            gram = mm_nt(kb, kb)
            score = mm_nt(qb, kb)
            kt = kn.T.astype(BF16)
            for d in range(2):
                r = d * chunks + n
                work.append(dict(d=d, r=r, n=n, qn=qn, kb=kb, v=v, kt=kt, gram=gram, score=score))
        for w in work:
            d, r = w["d"], w["r"]
            keep = (row >= col) if d == 0 else (row <= col)
            strict = (row > col) if d == 0 else (row < col)
            diff = col_ref[0, r] - row_ref[0, pl.ds(r, 1), :]
            within = jnp.where(keep, jnp.exp(jnp.where(keep, diff, 0.0)), 0.0)
            a = jnp.where(strict, w["gram"] * within * col_ref[1, r], 0.0).astype(BF16)
            w["a"] = a
            w["p"] = (w["score"] * within).astype(BF16)
            w["t"] = eye - (a * mask_ref[d, 0]).astype(F32)
        for level in range(1, len(spans)):
            for w in work:
                w["tb"] = w["t"].astype(BF16)
                w["x"] = mm(w["a"] * mask_ref[w["d"], level], w["tb"]).astype(BF16)
            for w in work:
                w["t"] = w["t"] - mm(w["tb"], w["x"])
        for w in work:
            r = w["r"]
            fresh = mm((w["t"] * row_ref[1, pl.ds(r, 1), :]).astype(BF16), w["v"])
            fix = mm((w["t"] * row_ref[2, pl.ds(r, 1), :]).astype(BF16), w["kb"])
            w["uw"] = jnp.concatenate([fresh, fix], axis=1)
        for w in work:
            r, d, n = w["r"], w["d"], w["n"]
            pu = mm(w["p"], w["uw"].astype(BF16))
            w["local"] = pu[:, :dh]
            qeff_ref[r] = (w["qn"] * col_ref[2, r] - pu[:, dh:]).astype(BF16)
            faded = col_ref[3, r]
            bk = mm(w["kt"], (w["uw"] * jnp.concatenate([faded, faded], axis=1)).astype(BF16))
            add_ref[r] = bk[:, :dh]
            cut_ref[r] = bk[:, dh:].astype(BF16)
        for u in range(PAIRED):
            n = step * PAIRED + u
            here = pl.ds(pl.multiple_of(n * C, C), C)
            out_ref[here, :] = work[2 * u]["local"] + work[2 * u + 1]["local"]
        return carry

    lax.fori_loop(0, chunks // PAIRED, body, 0)

    z = [jnp.concatenate([jnp.zeros((dh, dh), F32), eye], axis=1) for _ in range(2)]
    for step in range(chunks):
        for d in range(2):
            n = step if d == 0 else chunks - 1 - step
            r = d * chunks + n
            zb = z[d].astype(BF16)
            seen = mm(qeff_ref[r], zb)
            out_ref[n * C:(n + 1) * C, :] += seen[:, :dh]
            reach_ref[n * C:(n + 1) * C, d * dh:(d + 1) * dh] = seen[:, dh:].astype(BF16)
            keep = row_ref[3, r:r + 1, :]
            moved = mm(cut_ref[r], zb)
            z[d] = jnp.concatenate([z[d][:, :dh] * keep - moved[:, :dh] + add_ref[r],
                                    z[d][:, dh:] * keep - moved[:, dh:]], axis=1)
    for d in range(2):
        maps_ref[d] = z[d].astype(BF16)


def local_attention(q, k, v, rate, pre, shock, bpre):
    length, dh = q.shape
    chunks = length // CHUNK
    levels = CHUNK.bit_length() - 1
    vm = pl.BlockSpec(memory_space=pltpu.VMEM)
    return pl.pallas_call(
        local_kernel,
        out_shape=(
            jax.ShapeDtypeStruct((length, dh), F32),
            jax.ShapeDtypeStruct((length, 2 * dh), BF16),
            jax.ShapeDtypeStruct((2, dh, 2 * dh), BF16),
        ),
        in_specs=[pl.BlockSpec(memory_space=pltpu.SMEM)] + [vm] * 6,
        out_specs=(vm, vm, vm),
        scratch_shapes=[
            pltpu.VMEM((2, levels, CHUNK, CHUNK), BF16),
            pltpu.VMEM((4, 2 * chunks, CHUNK), F32),
            pltpu.VMEM((4, 2 * chunks, CHUNK, CHUNK), F32),
            pltpu.VMEM((2 * chunks, CHUNK, dh), BF16),
            pltpu.VMEM((2 * chunks, dh, dh), F32),
            pltpu.VMEM((2 * chunks, dh, dh), BF16),
        ],
        name="local_attention",
    )(rate, q, k, v, pre, shock, bpre)


def compose_kernel(where_ref, own_ref, one_ref, two_ref, three_ref, before_ref, all_ref, line_ref):
    dh = own_ref.shape[1]
    here = where_ref[0]
    for distance, ref in enumerate((own_ref, one_ref, two_ref, three_ref)):
        line_ref[lax.rem(here + 4 - distance, 4)] = ref[...]
    zero = jnp.concatenate(
        [jnp.zeros((dh, dh), F32), (iota2((dh, dh), 0) == iota2((dh, dh), 1)).astype(F32)], axis=1
    )
    for d in range(2):
        z = zero
        before = zero
        order = range(4) if d == 0 else range(3, -1, -1)
        for step, j in enumerate(order):
            before = jnp.where(here == j, z, before)
            added = line_ref[j, d, :, :dh].astype(F32)
            if step == 0:
                z = line_ref[j, d].astype(F32)
            else:
                moved = mm(line_ref[j, d, :, dh:], z.astype(BF16))
                z = jnp.concatenate([moved[:, :dh] + added, moved[:, dh:]], axis=1)
        before_ref[d] = before.astype(BF16)
        all_ref[d] = z.astype(BF16)


def compose_line(where, own, others):
    vm = pl.BlockSpec(memory_space=pltpu.VMEM)
    return pl.pallas_call(
        compose_kernel,
        out_shape=(jax.ShapeDtypeStruct(own.shape, BF16), jax.ShapeDtypeStruct(own.shape, BF16)),
        in_specs=[pl.BlockSpec(memory_space=pltpu.SMEM)] + [vm] * 4,
        out_specs=(vm, vm),
        scratch_shapes=[pltpu.VMEM((4,) + own.shape, BF16)],
        name="compose_line",
    )(where, own, *others)


def mix_kernel(where_ref, before_ref, own_ref, one_ref, two_ref, three_ref, local_ref, reach_ref,
               gate_ref, gain_ref, mixed_ref, line_ref, state_ref):
    dh = local_ref.shape[1]
    here = where_ref[0]
    for distance, ref in enumerate((own_ref, one_ref, two_ref, three_ref)):
        line_ref[lax.rem(here + 4 - distance, 4)] = ref[...]
    for d in range(2):
        s = jnp.zeros((dh, dh), F32)
        order = (0, 1, 2) if d == 0 else (3, 2, 1)
        for step, j in enumerate(order):
            passed = (j < here) if d == 0 else (j > here)
            added = line_ref[j, d, :, :dh].astype(F32)
            if step == 0:
                new = added
            else:
                new = mm(line_ref[j, d, :, dh:], s.astype(BF16)) + added
            s = jnp.where(passed, new, s)
        s = mm(before_ref[d, :, dh:], s.astype(BF16)) + before_ref[d, :, :dh].astype(F32)
        state_ref[d * dh:(d + 1) * dh, :] = s.astype(BF16)
    gain = gain_ref[...]
    block = 256
    for i in range(local_ref.shape[0] // block):
        here_rows = slice(i * block, (i + 1) * block)
        joined = local_ref[here_rows, :] + mm(reach_ref[here_rows, :], state_ref[...])
        gate = gate_ref[here_rows, :].astype(F32)
        gate = gate / (1.0 + jnp.exp(-gate))
        mean = jnp.mean(joined * joined, axis=1, keepdims=True)
        mixed_ref[here_rows, :] = (joined * lax.rsqrt(mean + EPS) * gain * gate).astype(BF16)


def mix_heads(where, before, own, others, local, reach, gate, gain):
    vm = pl.BlockSpec(memory_space=pltpu.VMEM)
    dh = local.shape[1]
    return pl.pallas_call(
        mix_kernel,
        out_shape=jax.ShapeDtypeStruct(local.shape, BF16),
        in_specs=[pl.BlockSpec(memory_space=pltpu.SMEM)] + [vm] * 9,
        out_specs=vm,
        scratch_shapes=[pltpu.VMEM((4,) + own.shape, BF16), pltpu.VMEM((2 * dh, dh), BF16)],
        name="mix_heads",
    )(where, before, own, *others, local, reach, gate, gain)


def project_kernel(own_ref, one_ref, two_ref, three_ref, w_ref, o0, o1, o2, o3):
    rows = own_ref.shape[0]
    stacked = jnp.concatenate([own_ref[...], one_ref[...], two_ref[...], three_ref[...]], axis=0)
    parts = mm(stacked, w_ref[...]).astype(BF16)
    for i, ref in enumerate((o0, o1, o2, o3)):
        ref[...] = parts[i * rows:(i + 1) * rows]


def project(blocks, weight):
    vm = pl.BlockSpec(memory_space=pltpu.VMEM)
    shape = jax.ShapeDtypeStruct((blocks[0].shape[0], weight.shape[1]), BF16)
    return pl.pallas_call(
        project_kernel, out_shape=(shape,) * 4, in_specs=[vm] * 5, out_specs=(vm,) * 4,
        name="project",
    )(*blocks, weight)


def route_kernel(where_ref, p0, p1, p2, p3, tokens_ref, gain_ref, slots_ref, residual_ref, outgoing_ref, line_ref):
    here = where_ref[0]
    for distance, ref in enumerate((p0, p1, p2, p3)):
        line_ref[lax.rem(here + distance, 4)] = ref[...]
    branch = jnp.concatenate([line_ref[j] for j in range(4)], axis=1).astype(F32)
    residual = tokens_ref[...].astype(F32) + branch
    residual_ref[...] = residual
    mean = jnp.mean(residual * residual, axis=1, keepdims=True)
    normed = (residual * lax.rsqrt(mean + EPS) * gain_ref[...]).astype(BF16)
    count = outgoing_ref.shape[0]
    slot = iota2((count, residual.shape[0]), 0)
    chooser = ((slot == slots_ref[0:1, :]) | (slot == slots_ref[1:2, :])).astype(F32).astype(BF16)
    outgoing_ref[...] = mm(chooser, normed).astype(BF16)


def route(where, parts, tokens, gain, slots, count):
    vm = pl.BlockSpec(memory_space=pltpu.VMEM)
    return pl.pallas_call(
        route_kernel,
        out_shape=(
            jax.ShapeDtypeStruct(tokens.shape, F32),
            jax.ShapeDtypeStruct((count, tokens.shape[1]), BF16),
        ),
        in_specs=[pl.BlockSpec(memory_space=pltpu.SMEM)] + [vm] * 7,
        out_specs=(vm, vm),
        scratch_shapes=[pltpu.VMEM((4,) + parts[0].shape, BF16)],
        name="route",
    )(where, *parts, tokens, gain, slots)


def expert_kernel(rows_ref, w_ref, out_ref, sum_ref):
    j = pl.program_id(0)

    @pl.when(j == 0)
    def _():
        sum_ref[...] = jnp.zeros_like(sum_ref)

    width = w_ref.shape[3]
    both = mm(rows_ref[...], jnp.concatenate([w_ref[0, 0], w_ref[0, 1]], axis=1))
    gate = both[:, :width]
    hidden = (gate / (1.0 + jnp.exp(-gate)) * both[:, width:]).astype(BF16)
    sum_ref[...] += mm_nt(hidden, w_ref[0, 2])

    @pl.when(j == pl.num_programs(0) - 1)
    def _():
        out_ref[...] = sum_ref[...].astype(BF16)


def run_expert(rows, weights):
    count, _, width, part = weights.shape
    return pl.pallas_call(
        expert_kernel,
        out_shape=jax.ShapeDtypeStruct(rows.shape, BF16),
        grid=(count,),
        in_specs=[
            pl.BlockSpec(rows.shape, lambda j: (0, 0)),
            pl.BlockSpec((1, 3, width, part), lambda j: (j, 0, 0, 0)),
        ],
        out_specs=pl.BlockSpec(rows.shape, lambda j: (0, 0)),
        scratch_shapes=[pltpu.VMEM(rows.shape, F32)],
        compiler_params=pltpu.CompilerParams(dimension_semantics=("arbitrary",)),
        name="run_expert",
    )(rows, weights)


def finish_kernel(residual_ref, rows_ref, slots_ref, weight_ref, out_ref):
    tokens = residual_ref.shape[0]
    count = rows_ref.shape[0]
    slot = iota2((tokens, count), 1)
    chosen = jnp.where(slot == slots_ref[:, 0:1], weight_ref[:, 0:1], 0.0) + jnp.where(
        slot == slots_ref[:, 1:2], weight_ref[:, 1:2], 0.0
    )
    high = chosen.astype(BF16)
    low = (chosen - high.astype(F32)).astype(BF16)
    rows = rows_ref[...]
    out_ref[...] = (residual_ref[...] + (mm(high, rows) + mm(low, rows))).astype(BF16)


def finish(residual, rows, slots, weight):
    vm = pl.BlockSpec(memory_space=pltpu.VMEM)
    return pl.pallas_call(
        finish_kernel,
        out_shape=jax.ShapeDtypeStruct(residual.shape, BF16),
        in_specs=[vm] * 4,
        out_specs=vm,
        name="finish",
    )(residual, rows, slots, weight)


def around(x, axis):
    size = lax.axis_size(axis)
    return [lax.ppermute(x, axis, [(i, (i + d) % size) for i in range(size)]) for d in range(1, size)]


def shards(
    query_vectors, key_vectors, value_vectors, out_gate, decay_rate, decay_pre, decay_shock, beta_pre,
    head_gain, w_out, tokens, norm_gain, experts_pick, pair_logits, group_logits,
    expert_gate, expert_up, expert_down,
):
    length, _, dh = query_vectors.shape
    chunks = length // CHUNK
    at_x = lax.axis_index("sp_1")
    at_y = lax.axis_index("sp_0")
    where_x = at_x.astype(jnp.int32).reshape(1)
    where_y = at_y.astype(jnp.int32).reshape(1)

    quarter = w_out.shape[1] // lax.axis_size("sp_1")
    w_part = lax.dynamic_slice_in_dim(w_out, at_x * quarter, quarter, 1)
    w_columns = lax.all_gather(w_part, "tp", axis=0, tiled=True)
    experts = jnp.concatenate([expert_gate, expert_up, expert_down], axis=0)
    experts, w_columns = lax.optimization_barrier((experts, w_columns)) if False else (experts, w_columns)
    expert_all = lax.all_gather(experts, "tp", axis=0)

    local_rows = tokens.shape[0]
    group_count = group_logits.shape[1]
    group_exp = jnp.exp(group_logits)
    group_share = group_exp / jnp.sum(group_exp, axis=-1, keepdims=True)
    group_index_of = experts_pick[:, 0] // GROUP_SIZE
    group_weight = jnp.sum(
        jnp.where(jnp.arange(group_count)[None, :] == group_index_of[:, None], group_share, 0.0), axis=1
    )
    pair_exp = jnp.exp(pair_logits)
    route_weight = pair_exp / jnp.sum(pair_exp, axis=-1, keepdims=True) * group_weight[:, None]
    capacity = local_rows // group_count
    expert_count = lax.axis_size(SP)
    expert_marks = jnp.sum(
        (experts_pick[:, :, None] == jnp.arange(expert_count, dtype=jnp.int32)[None, None, :]).astype(jnp.int32),
        axis=1,
    )
    before_me = (jnp.arange(local_rows)[None, :] < jnp.arange(local_rows)[:, None]).astype(BF16)
    earlier = jnp.dot(before_me, expert_marks.astype(BF16), preferred_element_type=F32).astype(jnp.int32)
    slot_in = jnp.sum(
        jnp.where(
            experts_pick[:, :, None] == jnp.arange(expert_count, dtype=jnp.int32)[None, None, :],
            earlier[:, None, :], 0,
        ),
        axis=2,
    )
    slot_place = experts_pick * capacity + slot_in

    local, reach, maps = local_attention(
        query_vectors.reshape(length, dh), key_vectors.reshape(length, dh), value_vectors.reshape(length, dh),
        decay_rate,
        decay_pre.reshape(2 * chunks, CHUNK), decay_shock.reshape(2 * chunks, CHUNK),
        beta_pre.reshape(2 * chunks, CHUNK),
    )
    before, line = compose_line(where_x, maps, around(maps, "sp_1"))
    mixed = mix_heads(
        where_y, before, line, around(line, "sp_0"), local, reach,
        out_gate.reshape(length, dh), head_gain.reshape(1, dh),
    )
    mine = lax.all_to_all(mixed, "tp", split_axis=0, concat_axis=1, tiled=True)
    parts = project([mine] + around(mine, "sp_1"), w_columns)
    size = lax.axis_size("sp_1")
    returned = [parts[0]] + [
        lax.ppermute(parts[d], "sp_1", [(i, (i - d) % size) for i in range(size)]) for d in range(1, size)
    ]
    residual, outgoing = route(
        where_x, returned, tokens, norm_gain.reshape(1, -1), slot_place.T, expert_count * capacity
    )
    width = outgoing.shape[1]
    outgoing = outgoing.reshape(expert_count, capacity, width)
    arrived = lax.all_to_all(outgoing, SP, split_axis=0, concat_axis=0, tiled=True)
    expert_rows = run_expert(arrived.reshape(expert_count * capacity, width), expert_all)
    expert_rows = expert_rows.reshape(expert_count, capacity, width)
    results = lax.all_to_all(expert_rows, SP, split_axis=0, concat_axis=0, tiled=True)
    return finish(residual, results.reshape(expert_count * capacity, width), slot_place, route_weight)


def solution(mesh):
    finer = Mesh(mesh.devices.reshape(4, 4, mesh.shape["tp"]), ("sp_0", "sp_1", "tp"))
    in_specs = (
        P(SP, "tp", None), P(SP, "tp", None), P(SP, "tp", None), P(SP, "tp", None),
        P(None, "tp"),
        P(None, "tp", SP), P(None, "tp", SP), P(None, "tp", SP),
        P(), P("tp", None), P(SP_TP, None), P(),
        P(SP_TP, None), P(SP_TP, None), P(SP_TP, None),
        P(SP, None, "tp"), P(SP, None, "tp"), P(SP, None, "tp"),
    )
    return jax.shard_map(
        shards, mesh=finer, in_specs=in_specs, out_specs=P(SP_TP, None), check_vma=False
    )
```

time: 682 us -> 242 us (0.35); the launches traced: 673 us -> 241 us
  other arithmetic: 171 us -> 4.05 us
  matrix products: 132 us -> 0.13 us
  blocking collectives: 90.5 us -> 0 us
  waiting for transfers between devices: 212 us -> 127 us
  Pallas kernels: 0 us -> 48.9 us
  local copies, waits for them, and re-layouts: 46 us -> 7.36 us
  starting transfers between devices: 6.62 us -> 39.9 us
    another operation x10 -> x0, other arithmetic: 159 us -> none  [the longest x5 158 us: block_sweep(): jax.scipy.linalg.solve_triangular(lower_matrix + identity, right_side, lo...]
    reduce_scatter x2 -> x0, waiting for transfers between devices: 147 us -> none  [the longest x1 81.1 us: shards(): lax.psum_scatter(lax.optimization_barrier(part_sum).astype(jnp.float32).a...]
    dot_general x163 -> x1, matrix products: 128 us -> 0.13 us  [shards(): jnp.dot(before_me, expert_marks.astype(BF16), preferred_element_type=F32)]
    all_gather x8 -> x0, blocking collectives: 75.2 us -> none  [prefix_by_axis(): lax.all_gather(part.astype(kind), axis)]
    pallas_call x0 -> x7, Pallas kernels: none -> 48.9 us  [the longest x1 20.2 us: run_expert(): pl.pallas_call(expert_kernel, out_shape=jax.ShapeDtypeStruct(rows.shape,...]
    ppermute x0 -> x12, waiting for transfers between devices: none -> 24.7 us  [the longest x9 20.1 us: around(): lax.ppermute(x, axis, [(i, (i + d) % size) for i in range(size)])]
    all_to_all x0 -> x2, waiting for transfers between devices: none -> 24.5 us  [the longest x1 14.3 us: shards(): mine = lax.all_to_all(mixed, 'tp', split_axis=0, concat_axis=1, tiled=True)]
    exp x32 -> x0, local copies, waits for them, and re-layouts: 18.5 us -> none  [advance(): carried = carried * jnp.exp(total_in) + jnp.dot(key_in.T, updated)]
  transfers between devices with their start and end apart: 4 -> 17, of which waited for: 4 -> 15; matrix products, arithmetic and copies ran while one was open for 0% -> 2% of each run, Pallas kernels for 0% -> 11%
where the time goes in v1:
time: 242 us; the launch traced here: 241 us
  waiting for transfers between devices  127 us (52%)
  Pallas kernels  48.9 us (20%)
  starting transfers between devices  39.9 us (16%)
  between operations  13.5 us (6%)
  local copies, waits for them, and re-layouts  7.36 us (3%)
  other arithmetic  4.05 us (2%)
    all_gather x1, waiting for transfers between devices, shards(): expert_all = lax.all_gather(experts, 'tp', axis=0)  68.8 us
    pallas_call x1, Pallas kernels, run_expert(): pl.pallas_call(expert_kernel, out_shape=jax.ShapeDtypeStruct(rows.shape,...  20.2 us
    ppermute x9, waiting for transfers between devices, around(): lax.ppermute(x, axis, [(i, (i + d) % size) for i in range(size)])  20.1 us
    pallas_call x1, Pallas kernels, local_attention(): pl.pallas_call(local_kernel, out_shape=(jax.ShapeDtypeStruct((length, dh)...  14.9 us
    ppermute x9, starting transfers between devices, around(): lax.ppermute(x, axis, [(i, (i + d) % size) for i in range(size)])  14.8 us
    all_to_all x1, waiting for transfers between devices, shards(): mine = lax.all_to_all(mixed, 'tp', split_axis=0, concat_axis=1, tiled=True)  14.3 us
    all_to_all x1, starting transfers between devices, shards(): mine = lax.all_to_all(mixed, 'tp', split_axis=0, concat_axis=1, tiled=True)  10.8 us
    all_to_all x1, waiting for transfers between devices, shards(): lax.all_to_all(outgoing, SP, split_axis=0, concat_axis=0, tiled=True)  10.2 us
  transfers between devices with their start and end apart: 17, of which 15 were waited for; matrix products, arithmetic and copies ran while one was open for 2% of the time, Pallas kernels for 11%

profile of v1, /device:TPU:1, one launch (start us, length us, event | category | flops | bytes accessed | tf_op | source)
XLA Modules:
  0.0 241.1 jit_solution(9448507740373467638)
XLA Ops:
  6.5 0.0 copy-start
  6.5 1.0 copy-done
  7.6 0.7 constant_dynamic-slice_fusion
  8.2 0.0 all-gather.4.cloned.1.call-update
  8.3 0.0 all-gather.6.cloned.1.call-start
  8.3 2.7 %pad_maximum_fusion = bf16[3,2048,128]{2,1,0:T(8,128)(2,1)} fusion(bf16[1,2048,128]{2,1,0:T(8,128)(2,1)} %param.35, bf16[1,2048,128]{2,1,0:T(8,128)(2,1)} %param.34, bf16[1,2048,128]{2,1,0:T(8,128)(2,1)} %param.33), kind=kLoop, calls=%fused_computation | loop fusion | flops 1572864 | bytes 3145728 | tf_op jit(solution)/shard_map/concatenate | solution.py:386
  11.0 0.0 all-gather.6.cloned.1.call-update
  11.0 0.6 copy-done.20
  11.6 0.7 copy.48.rate_ref
  12.3 14.9 %local_attention.1 = (f32[1024,128]{1,0:T(8,128)}, bf16[1024,256]{1,0:T(8,128)(2,1)}, bf16[2,128,256]{2,1,0:T(8,128)(2,1)}) custom-call(f32[2,1]{1,0:T(2,128)} %copy.48.rate_ref, bf16[1024,128]{1,0:T(8,128)(2,1)} %bitcast.32, bf16[1024,128]{1,0:T(8,128)(2,1)} %bitcast.33, bf16[1024,128]{1,0:T(8,128)(2,1)} %bitcast.34, f32[16,128]{1,0:T(8,128)} %bitcast.37, ...), custom_call_target="tpu_custom_call" | custom-call | tf_op jit(solution)/shard_map/local_attention/pallas_call | solution.py:160
  27.2 2.0 collective-permute-start
  29.2 2.5 %collective-permute-start.1 = (bf16[2,128,256]{2,1,0:T(8,128)(2,1)}, bf16[2,128,256]{2,1,0:T(8,128)(2,1)S(1)}, u32[]{:S(2)}, u32[]{:S(2)}) collective-permute-start(bf16[2,128,256]{2,1,0:T(8,128)(2,1)} %get-tuple-element.16.own_ref), channel_id=1, source_target_pairs={{0,32},{16,48},{32,0},{48,16},{1,33},{17,49},{33,1},{49,17},{2,34}... | collective-permute-start | bytes 393224 | tf_op jit(solution)/shard_map/ppermute | solution.py:368
  31.7 1.1 collective-permute-start.2
  32.8 0.3 collective-permute-done.one_ref
  33.1 4.5 %collective-permute-done.1.two_ref = bf16[2,128,256]{2,1,0:T(8,128)(2,1)S(1)} collective-permute-done((bf16[2,128,256]{2,1,0:T(8,128)(2,1)}, bf16[2,128,256]{2,1,0:T(8,128)(2,1)S(1)}, u32[]{:S(2)}, u32[]{:S(2)}) %collective-permute-start.1) | collective-permute-done | bytes 131104 | tf_op jit(solution)/shard_map/ppermute | solution.py:368
  37.6 0.0 collective-permute-done.2.three_ref
  37.6 0.0 copy-done.10
  37.6 0.6 copy-done.11
  38.3 0.0 copy-done.12
  38.3 2.4 %compose_line.1 = (bf16[2,128,256]{2,1,0:T(8,128)(2,1)}, bf16[2,128,256]{2,1,0:T(8,128)(2,1)}) custom-call(s32[1]{0:T(128)} %bitcast.where_ref, bf16[2,128,256]{2,1,0:T(8,128)(2,1)} %get-tuple-element.16.own_ref, bf16[2,128,256]{2,1,0:T(8,128)(2,1)} %copy-done.10, bf16[2,128,256]{2,1,0:T(8,128)(2,1)} %copy-done.11, bf16[2,128,256]{2,1,0:T(8,128)(2,1)} %copy-done.12), custom_call_target="tpu_custom_call" | custom-call | tf_op jit(solution)/shard_map/compose_line/pallas_call | solution.py:207
  40.7 1.3 collective-permute-start.3
  42.0 2.6 %collective-permute-start.4 = (bf16[2,128,256]{2,1,0:T(8,128)(2,1)}, bf16[2,128,256]{2,1,0:T(8,128)(2,1)S(1)}, u32[]{:S(2)}, u32[]{:S(2)}) collective-permute-start(bf16[2,128,256]{2,1,0:T(8,128)(2,1)} %get-tuple-element.18.own_ref), channel_id=1, source_target_pairs={{0,128},{64,192},{128,0},{192,64},{1,129},{65,193},{129,1},{193,65... | collective-permute-start | bytes 393224 | tf_op jit(solution)/shard_map/ppermute | solution.py:368
  44.7 1.1 collective-permute-start.5
  45.7 0.3 collective-permute-done.3.one_ref
  46.1 3.5 %collective-permute-done.4.two_ref = bf16[2,128,256]{2,1,0:T(8,128)(2,1)S(1)} collective-permute-done((bf16[2,128,256]{2,1,0:T(8,128)(2,1)}, bf16[2,128,256]{2,1,0:T(8,128)(2,1)S(1)}, u32[]{:S(2)}, u32[]{:S(2)}) %collective-permute-start.4) | collective-permute-done | bytes 131104 | tf_op jit(solution)/shard_map/ppermute | solution.py:368
  49.5 0.4 collective-permute-done.5.three_ref
  49.9 0.3 copy-done.8
  50.2 0.4 copy-done.9
  50.6 3.3 %mix_heads.1 = bf16[1024,128]{1,0:T(8,128)(2,1)} custom-call(s32[1]{0:T(128)} %bitcast.1.where_ref, bf16[2,128,256]{2,1,0:T(8,128)(2,1)} %get-tuple-element.17.before_ref, bf16[2,128,256]{2,1,0:T(8,128)(2,1)} %get-tuple-element.18.own_ref, bf16[2,128,256]{2,1,0:T(8,128)(2,1)} %copy-done.7, bf16[2,128,256]{2,1,0:T(8,128)(2,1)} %copy-done.8, ...), custom_call_target="tpu_custom_call" | custom-call | tf_op jit(solution)/shard_map/mix_heads/pallas_call | solution.py:250
  53.8 10.8 %all-to-all-start = ((bf16[16,64,128]{2,1,0:T(8,128)(2,1)}), bf16[16,64,128]{2,1,0:T(8,128)(2,1)S(1)}, u32[]{:S(2)}, u32[]{:S(2)}) async-start(bf16[16,64,128]{2,1,0:T(8,128)(2,1)} %bitcast.30), calls=%async_computation | async-start | bytes 524288 | tf_op jit(solution)/shard_map/all_to_all | solution.py:428
  64.6 14.3 %all-to-all-done = bf16[16,64,128]{2,1,0:T(8,128)(2,1)S(1)} async-done(((bf16[16,64,128]{2,1,0:T(8,128)(2,1)}), bf16[16,64,128]{2,1,0:T(8,128)(2,1)S(1)}, u32[]{:S(2)}, u32[]{:S(2)}) %all-to-all-start) | async-done | bytes 262176 | tf_op jit(solution)/shard_map/all_to_all | solution.py:428
  79.0 0.0 copy-start.3
  79.0 1.7 collective-permute-start.6
  80.7 1.8 collective-permute-start.7
  82.5 0.7 collective-permute-start.8
  83.2 0.1 convolution_convert_fusion
  83.3 5.2 %collective-permute-done.6.one_ref = bf16[64,2048]{1,0:T(8,128)(2,1)S(1)} collective-permute-done((bf16[64,2048]{1,0:T(8,128)(2,1)S(1)}, bf16[64,2048]{1,0:T(8,128)(2,1)S(1)}, u32[]{:S(2)}, u32[]{:S(2)}) %collective-permute-start.6) | collective-permute-done | bytes 262176 | tf_op jit(solution)/shard_map/ppermute | solution.py:368
  88.5 5.8 %collective-permute-done.7.two_ref = bf16[64,2048]{1,0:T(8,128)(2,1)S(1)} collective-permute-done((bf16[64,2048]{1,0:T(8,128)(2,1)S(1)}, bf16[64,2048]{1,0:T(8,128)(2,1)S(1)}, u32[]{:S(2)}, u32[]{:S(2)}) %collective-permute-start.7) | collective-permute-done | bytes 262176 | tf_op jit(solution)/shard_map/ppermute | solution.py:368
  94.4 0.1 collective-permute-done.8.three_ref
  94.5 0.6 copy-done.5
  95.1 0.2 copy-done.6
  95.2 3.4 %project.1 = (bf16[64,512]{1,0:T(8,128)(2,1)}, bf16[64,512]{1,0:T(8,128)(2,1)}, bf16[64,512]{1,0:T(8,128)(2,1)}, bf16[64,512]{1,0:T(8,128)(2,1)}) custom-call(bf16[64,2048]{1,0:T(8,128)(2,1)} %copy-done.3, bf16[64,2048]{1,0:T(8,128)(2,1)} %copy-done.4, bf16[64,2048]{1,0:T(8,128)(2,1)} %copy-done.5, bf16[64,2048]{1,0:T(8,128)(2,1)} %copy-done.6, ...), custom_call_target="tpu_custom_call" | custom-call | tf_op jit(solution)/shard_map/project/pallas_call | solution.py:271
  98.6 2.7 %collective-permute-start.9 = (bf16[64,512]{1,0:T(8,128)(2,1)}, bf16[64,512]{1,0:T(8,128)(2,1)S(1)}, u32[]{:S(2)}, u32[]{:S(2)}) collective-permute-start(bf16[64,512]{1,0:T(8,128)(2,1)} %get-tuple-element.22), channel_id=1, source_target_pairs={{0,48},{16,0},{32,16},{48,32},{1,49},{17,1},{33,17},{49,33},{2,50}... | collective-permute-start | bytes 196616 | tf_op jit(solution)/shard_map/ppermute | solution.py:432
  101.3 0.9 collective-permute-start.10
  102.1 0.0 collective-permute-start.11
  102.1 0.6 multiply_add_fusion
  102.7 0.2 collective-permute-done.9.p1
  103.0 3.2 %collective-permute-done.10.p2 = bf16[64,512]{1,0:T(8,128)(2,1)S(1)} collective-permute-done((bf16[64,512]{1,0:T(8,128)(2,1)}, bf16[64,512]{1,0:T(8,128)(2,1)S(1)}, u32[]{:S(2)}, u32[]{:S(2)}) %collective-permute-start.10) | collective-permute-done | bytes 65568 | tf_op jit(solution)/shard_map/ppermute | solution.py:432
  106.1 1.2 collective-permute-done.11.p3
  107.3 0.6 copy-done.15
  108.0 2.4 route.1
  110.3 4.7 %all-to-all-start.1 = ((bf16[16,8,2048]{2,1,0:T(8,128)(2,1)}), bf16[16,8,2048]{2,1,0:T(8,128)(2,1)S(1)}, u32[]{:S(2)}, u32[]{:S(2)}) async-start(bf16[16,8,2048]{2,1,0:T(8,128)(2,1)} %bitcast.31), calls=%async_computation.1 | async-start | bytes 1048576 | tf_op jit(solution)/shard_map/all_to_all | solution.py:439
  115.0 0.0 copy-done.19
  115.1 10.2 %all-to-all-done.1 = bf16[16,8,2048]{2,1,0:T(8,128)(2,1)S(1)} async-done(((bf16[16,8,2048]{2,1,0:T(8,128)(2,1)}), bf16[16,8,2048]{2,1,0:T(8,128)(2,1)S(1)}, u32[]{:S(2)}, u32[]{:S(2)}) %all-to-all-start.1) | async-done | bytes 524320 | tf_op jit(solution)/shard_map/all_to_all | solution.py:439
  125.3 68.8 %all-gather.6.cloned.1.call-done = bf16[48,2048,128]{2,1,0:T(8,128)(2,1)} async-done(((bf16[3,2048,128]{2,1,0:T(8,128)(2,1)}), bf16[48,2048,128]{2,1,0:T(8,128)(2,1)}) %all-gather.6.cloned.1.call-update) | async-done | bytes 25165840 | tf_op jit(solution)/shard_map/all_gather | solution.py:388
  194.0 20.2 %run_expert.1 = bf16[128,2048]{1,0:T(8,128)(2,1)} custom-call(bf16[128,2048]{1,0:T(8,128)(2,1)} %bitcast.28, bf16[16,3,2048,128]{3,2,1,0:T(8,128)(2,1)} %bitcast.26), custom_call_target="tpu_custom_call" | custom-call | tf_op jit(solution)/shard_map/run_expert/pallas_call | solution.py:327
  214.3 6.1 %all-to-all-start.2 = ((bf16[16,8,2048]{2,1,0:T(8,128)(2,1)}), bf16[16,8,2048]{2,1,0:T(8,128)(2,1)S(1)}, u32[]{:S(2)}, u32[]{:S(2)}) async-start(bf16[16,8,2048]{2,1,0:T(8,128)(2,1)} %bitcast.27), calls=%async_computation.2 | async-start | bytes 1048576 | tf_op jit(solution)/shard_map/all_to_all | solution.py:442
  220.4 0.0 copy-done.17
  220.4 0.7 copy.53.slots_ref
  221.1 0.1 copy.51
  221.2 0.7 broadcast_multiply_fusion.weight_ref
  221.9 9.3 %all-to-all-done.2 = bf16[16,8,2048]{2,1,0:T(8,128)(2,1)S(1)} async-done(((bf16[16,8,2048]{2,1,0:T(8,128)(2,1)}), bf16[16,8,2048]{2,1,0:T(8,128)(2,1)S(1)}, u32[]{:S(2)}, u32[]{:S(2)}) %all-to-all-start.2) | async-done | bytes 524320 | tf_op jit(solution)/shard_map/all_to_all | solution.py:442
  231.2 0.8 copy-done.2
  232.0 2.3 finish.1
  (37 shorter events, 0.2 us)
Async XLA Ops:
  6.5 1.0 copy-start
  6.5 88.0 %all-gather.4.cloned.1.call-start = ((), (), s32[]{:S(2)}) async-start(), calls=%async_computation.3 | async-start | bytes 2228224 | tf_op jit(solution)/shard_map/all_gather | solution.py:385
  8.3 185.8 %all-gather.6.cloned.1.call-start = ((), (), s32[]{:S(2)}) async-start(), calls=%async_computation.4 | async-start | bytes 26738688 | tf_op jit(solution)/shard_map/all_gather | solution.py:388
  11.0 0.7 copy-start.20
  27.2 5.9 %collective-permute-start = (bf16[2,128,256]{2,1,0:T(8,128)(2,1)}, bf16[2,128,256]{2,1,0:T(8,128)(2,1)S(1)}, u32[]{:S(2)}, u32[]{:S(2)}) collective-permute-start(bf16[2,128,256]{2,1,0:T(8,128)(2,1)} %get-tuple-element.16.own_ref), channel_id=1, source_target_pairs={{0,16},{16,32},{32,48},{48,0},{1,17},{17,33},{33,49},{49,1},{2,18}... | collective-permute-start | bytes 393224 | tf_op jit(solution)/shard_map/ppermute | solution.py:368
  29.2 8.4 %collective-permute-start.1 = (bf16[2,128,256]{2,1,0:T(8,128)(2,1)}, bf16[2,128,256]{2,1,0:T(8,128)(2,1)S(1)}, u32[]{:S(2)}, u32[]{:S(2)}) collective-permute-start(bf16[2,128,256]{2,1,0:T(8,128)(2,1)} %get-tuple-element.16.own_ref), channel_id=1, source_target_pairs={{0,32},{16,48},{32,0},{48,16},{1,33},{17,49},{33,1},{49,17},{2,34}... | collective-permute-start | bytes 393224 | tf_op jit(solution)/shard_map/ppermute | solution.py:368
  31.7 5.9 %collective-permute-start.2 = (bf16[2,128,256]{2,1,0:T(8,128)(2,1)}, bf16[2,128,256]{2,1,0:T(8,128)(2,1)S(1)}, u32[]{:S(2)}, u32[]{:S(2)}) collective-permute-start(bf16[2,128,256]{2,1,0:T(8,128)(2,1)} %get-tuple-element.16.own_ref), channel_id=1, source_target_pairs={{0,48},{16,0},{32,16},{48,32},{1,49},{17,1},{33,17},{49,33},{2,50}... | collective-permute-start | bytes 393224 | tf_op jit(solution)/shard_map/ppermute | solution.py:368
  33.1 4.5 %copy-start.10 = (bf16[2,128,256]{2,1,0:T(8,128)(2,1)}, bf16[2,128,256]{2,1,0:T(8,128)(2,1)S(1)}, u32[]{:S(2)}) copy-start(bf16[2,128,256]{2,1,0:T(8,128)(2,1)S(1)} %collective-permute-done.one_ref) | copy-start | bytes 393220
  37.6 0.7 copy-start.11
  37.6 0.7 copy-start.12
  38.3 26.3 %copy-start.18 = (s32[64,2]{0,1:T(2,128)S(1)}, s32[64,2]{0,1:T(2,128)}, u32[]{:S(2)}) copy-start(s32[64,2]{0,1:T(2,128)} %param.30) | copy-start | bytes 1540
  40.7 5.3 %collective-permute-start.3 = (bf16[2,128,256]{2,1,0:T(8,128)(2,1)}, bf16[2,128,256]{2,1,0:T(8,128)(2,1)S(1)}, u32[]{:S(2)}, u32[]{:S(2)}) collective-permute-start(bf16[2,128,256]{2,1,0:T(8,128)(2,1)} %get-tuple-element.18.own_ref), channel_id=1, source_target_pairs={{0,64},{64,128},{128,192},{192,0},{1,65},{65,129},{129,193},{193,1... | collective-permute-start | bytes 393224 | tf_op jit(solution)/shard_map/ppermute | solution.py:368
  42.0 7.5 %collective-permute-start.4 = (bf16[2,128,256]{2,1,0:T(8,128)(2,1)}, bf16[2,128,256]{2,1,0:T(8,128)(2,1)S(1)}, u32[]{:S(2)}, u32[]{:S(2)}) collective-permute-start(bf16[2,128,256]{2,1,0:T(8,128)(2,1)} %get-tuple-element.18.own_ref), channel_id=1, source_target_pairs={{0,128},{64,192},{128,0},{192,64},{1,129},{65,193},{129,1},{193,65... | collective-permute-start | bytes 393224 | tf_op jit(solution)/shard_map/ppermute | solution.py:368
  44.7 5.2 %collective-permute-start.5 = (bf16[2,128,256]{2,1,0:T(8,128)(2,1)}, bf16[2,128,256]{2,1,0:T(8,128)(2,1)S(1)}, u32[]{:S(2)}, u32[]{:S(2)}) collective-permute-start(bf16[2,128,256]{2,1,0:T(8,128)(2,1)} %get-tuple-element.18.own_ref), channel_id=1, source_target_pairs={{0,192},{64,0},{128,64},{192,128},{1,193},{65,1},{129,65},{193,129... | collective-permute-start | bytes 393224 | tf_op jit(solution)/shard_map/ppermute | solution.py:368
  46.0 3.9 %copy-start.7 = (bf16[2,128,256]{2,1,0:T(8,128)(2,1)}, bf16[2,128,256]{2,1,0:T(8,128)(2,1)S(1)}, u32[]{:S(2)}) copy-start(bf16[2,128,256]{2,1,0:T(8,128)(2,1)S(1)} %collective-permute-done.3.one_ref) | copy-start | bytes 393220
  49.5 0.7 copy-start.8
  49.9 0.7 copy-start.9
  53.8 25.1 %all-to-all-start = ((bf16[16,64,128]{2,1,0:T(8,128)(2,1)}), bf16[16,64,128]{2,1,0:T(8,128)(2,1)S(1)}, u32[]{:S(2)}, u32[]{:S(2)}) async-start(bf16[16,64,128]{2,1,0:T(8,128)(2,1)} %bitcast.30), calls=%async_computation | async-start | bytes 524288 | tf_op jit(solution)/shard_map/all_to_all | solution.py:428
  79.0 15.5 %copy-start.3 = (bf16[64,2048]{1,0:T(8,128)(2,1)}, bf16[64,2048]{1,0:T(8,128)(2,1)S(1)}, u32[]{:S(2)}) copy-start(bf16[64,2048]{1,0:T(8,128)(2,1)S(1)} %copy_bitcast_fusion.own_ref) | copy-start | bytes 786436
  79.0 9.6 %collective-permute-start.6 = (bf16[64,2048]{1,0:T(8,128)(2,1)S(1)}, bf16[64,2048]{1,0:T(8,128)(2,1)S(1)}, u32[]{:S(2)}, u32[]{:S(2)}) collective-permute-start(bf16[64,2048]{1,0:T(8,128)(2,1)S(1)} %copy_bitcast_fusion.own_ref), channel_id=1, source_target_pairs={{0,16},{16,32},{32,48},{48,0},{1,17},{17,33},{33,49},{49,1},{2,18}... | collective-permute-start | bytes 786440 | tf_op jit(solution)/shard_map/ppermute | solution.py:368
  80.7 13.7 %collective-permute-start.7 = (bf16[64,2048]{1,0:T(8,128)(2,1)S(1)}, bf16[64,2048]{1,0:T(8,128)(2,1)S(1)}, u32[]{:S(2)}, u32[]{:S(2)}) collective-permute-start(bf16[64,2048]{1,0:T(8,128)(2,1)S(1)} %copy_bitcast_fusion.own_ref), channel_id=1, source_target_pairs={{0,32},{16,48},{32,0},{48,16},{1,33},{17,49},{33,1},{49,17},{2,34}... | collective-permute-start | bytes 786440 | tf_op jit(solution)/shard_map/ppermute | solution.py:368
  82.5 12.0 %collective-permute-start.8 = (bf16[64,2048]{1,0:T(8,128)(2,1)S(1)}, bf16[64,2048]{1,0:T(8,128)(2,1)S(1)}, u32[]{:S(2)}, u32[]{:S(2)}) collective-permute-start(bf16[64,2048]{1,0:T(8,128)(2,1)S(1)} %copy_bitcast_fusion.own_ref), channel_id=1, source_target_pairs={{0,48},{16,0},{32,16},{48,32},{1,49},{17,1},{33,17},{49,33},{2,50}... | collective-permute-start | bytes 786440 | tf_op jit(solution)/shard_map/ppermute | solution.py:368
  88.5 6.0 %copy-start.4 = (bf16[64,2048]{1,0:T(8,128)(2,1)}, bf16[64,2048]{1,0:T(8,128)(2,1)S(1)}, u32[]{:S(2)}) copy-start(bf16[64,2048]{1,0:T(8,128)(2,1)S(1)} %collective-permute-done.6.one_ref) | copy-start | bytes 786436
  94.3 0.7 copy-start.5
  94.5 0.7 copy-start.6
  98.6 16.4 %copy-start.19 = (f32[64,2]{0,1:T(2,128)S(1)}, f32[64,2]{0,1:T(2,128)}, u32[]{:S(2)}) copy-start(f32[64,2]{0,1:T(2,128)} %param.31) | copy-start | bytes 1540
  98.6 4.4 %collective-permute-start.9 = (bf16[64,512]{1,0:T(8,128)(2,1)}, bf16[64,512]{1,0:T(8,128)(2,1)S(1)}, u32[]{:S(2)}, u32[]{:S(2)}) collective-permute-start(bf16[64,512]{1,0:T(8,128)(2,1)} %get-tuple-element.22), channel_id=1, source_target_pairs={{0,48},{16,0},{32,16},{48,32},{1,49},{17,1},{33,17},{49,33},{2,50}... | collective-permute-start | bytes 196616 | tf_op jit(solution)/shard_map/ppermute | solution.py:432
  101.3 4.9 %collective-permute-start.10 = (bf16[64,512]{1,0:T(8,128)(2,1)}, bf16[64,512]{1,0:T(8,128)(2,1)S(1)}, u32[]{:S(2)}, u32[]{:S(2)}) collective-permute-start(bf16[64,512]{1,0:T(8,128)(2,1)} %get-tuple-element.23), channel_id=1, source_target_pairs={{0,32},{16,48},{32,0},{48,16},{1,33},{17,49},{33,1},{49,17},{2,34}... | collective-permute-start | bytes 196616 | tf_op jit(solution)/shard_map/ppermute | solution.py:432
  102.1 5.2 %collective-permute-start.11 = (bf16[64,512]{1,0:T(8,128)(2,1)}, bf16[64,512]{1,0:T(8,128)(2,1)S(1)}, u32[]{:S(2)}, u32[]{:S(2)}) collective-permute-start(bf16[64,512]{1,0:T(8,128)(2,1)} %get-tuple-element.24), channel_id=1, source_target_pairs={{0,16},{16,32},{32,48},{48,0},{1,17},{17,33},{33,49},{49,1},{2,18}... | collective-permute-start | bytes 196616 | tf_op jit(solution)/shard_map/ppermute | solution.py:432
  102.9 4.4 %copy-start.13 = (bf16[64,512]{1,0:T(8,128)(2,1)}, bf16[64,512]{1,0:T(8,128)(2,1)S(1)}, u32[]{:S(2)}) copy-start(bf16[64,512]{1,0:T(8,128)(2,1)S(1)} %collective-permute-done.9.p1) | copy-start | bytes 196612
  106.1 1.2 copy-start.14
  107.3 0.6 copy-start.15
  110.3 14.9 %all-to-all-start.1 = ((bf16[16,8,2048]{2,1,0:T(8,128)(2,1)}), bf16[16,8,2048]{2,1,0:T(8,128)(2,1)S(1)}, u32[]{:S(2)}, u32[]{:S(2)}) async-start(bf16[16,8,2048]{2,1,0:T(8,128)(2,1)} %bitcast.31), calls=%async_computation.1 | async-start | bytes 1048576 | tf_op jit(solution)/shard_map/all_to_all | solution.py:439
  125.3 68.8 %copy-start.1 = (bf16[16,8,2048]{2,1,0:T(8,128)(2,1)}, bf16[16,8,2048]{2,1,0:T(8,128)(2,1)S(1)}, u32[]{:S(2)}) copy-start(bf16[16,8,2048]{2,1,0:T(8,128)(2,1)S(1)} %all-to-all-done.1) | copy-start | bytes 1572868
  194.0 26.3 %copy-start.17 = (s32[64,2]{0,1:T(2,128)S(1)}, s32[64,2]{0,1:T(2,128)}, u32[]{:S(2)}) copy-start(s32[64,2]{0,1:T(2,128)} %multiply_add_fusion) | copy-start | bytes 1540
  194.0 27.1 %copy-start.16 = (f32[64,8]{0,1:T(8,128)S(1)}, f32[64,8]{0,1:T(8,128)}, u32[]{:S(2)}) copy-start(f32[64,8]{0,1:T(8,128)} %param.32) | copy-start | bytes 6148
  214.3 16.9 %all-to-all-start.2 = ((bf16[16,8,2048]{2,1,0:T(8,128)(2,1)}), bf16[16,8,2048]{2,1,0:T(8,128)(2,1)S(1)}, u32[]{:S(2)}, u32[]{:S(2)}) async-start(bf16[16,8,2048]{2,1,0:T(8,128)(2,1)} %bitcast.27), calls=%async_computation.2 | async-start | bytes 1048576 | tf_op jit(solution)/shard_map/all_to_all | solution.py:442
  231.2 0.8 copy-start.2
Sparse Core Ops, SparseCore 0:
  9.2 43.5 all-gather.3
  54.5 139.4 all-gather.5

commit v2 on v1

--- a/solution.py
+++ b/solution.py
@@ -178,14 +178,16 @@
     )(rate, q, k, v, pre, shock, bpre)
 
 
-def compose_kernel(where_ref, own_ref, one_ref, two_ref, three_ref, before_ref, all_ref, line_ref):
+def compose_kernel(where_ref, own_ref, one_ref, two_ref, three_ref, before_ref, s1, s2, s3, line_ref):
     dh = own_ref.shape[1]
     here = where_ref[0]
+    across = where_ref[1]
     for distance, ref in enumerate((own_ref, one_ref, two_ref, three_ref)):
         line_ref[lax.rem(here + 4 - distance, 4)] = ref[...]
     zero = jnp.concatenate(
         [jnp.zeros((dh, dh), F32), (iota2((dh, dh), 0) == iota2((dh, dh), 1)).astype(F32)], axis=1
     )
+    ends = []
     for d in range(2):
         z = zero
         before = zero
@@ -199,37 +201,39 @@
                 moved = mm(line_ref[j, d, :, dh:], z.astype(BF16))
                 z = jnp.concatenate([moved[:, :dh] + added, moved[:, dh:]], axis=1)
         before_ref[d] = before.astype(BF16)
-        all_ref[d] = z.astype(BF16)
+        ends.append(z)
+    for distance, ref in enumerate((s1, s2, s3), 1):
+        ref[...] = jnp.where(across + distance < 4, ends[0], ends[1]).astype(BF16)
 
 
 def compose_line(where, own, others):
     vm = pl.BlockSpec(memory_space=pltpu.VMEM)
     return pl.pallas_call(
         compose_kernel,
-        out_shape=(jax.ShapeDtypeStruct(own.shape, BF16), jax.ShapeDtypeStruct(own.shape, BF16)),
+        out_shape=(jax.ShapeDtypeStruct(own.shape, BF16),) + (jax.ShapeDtypeStruct(own.shape[1:], BF16),) * 3,
         in_specs=[pl.BlockSpec(memory_space=pltpu.SMEM)] + [vm] * 4,
-        out_specs=(vm, vm),
+        out_specs=(vm,) * 4,
         scratch_shapes=[pltpu.VMEM((4,) + own.shape, BF16)],
         name="compose_line",
     )(where, own, *others)
 
 
-def mix_kernel(where_ref, before_ref, own_ref, one_ref, two_ref, three_ref, local_ref, reach_ref,
+def mix_kernel(where_ref, before_ref, one_ref, two_ref, three_ref, local_ref, reach_ref,
                gate_ref, gain_ref, mixed_ref, line_ref, state_ref):
     dh = local_ref.shape[1]
-    here = where_ref[0]
-    for distance, ref in enumerate((own_ref, one_ref, two_ref, three_ref)):
-        line_ref[lax.rem(here + 4 - distance, 4)] = ref[...]
+    here = where_ref[1]
+    for distance, ref in enumerate((one_ref, two_ref, three_ref), 1):
+        line_ref[distance] = ref[...]
+    line_ref[0] = jnp.zeros_like(one_ref)
     for d in range(2):
         s = jnp.zeros((dh, dh), F32)
         order = (0, 1, 2) if d == 0 else (3, 2, 1)
         for step, j in enumerate(order):
             passed = (j < here) if d == 0 else (j > here)
-            added = line_ref[j, d, :, :dh].astype(F32)
-            if step == 0:
-                new = added
-            else:
-                new = mm(line_ref[j, d, :, dh:], s.astype(BF16)) + added
+            piece = lax.rem(here - j + 4, 4)
+            new = line_ref[piece, :, :dh].astype(F32)
+            if step > 0:
+                new = new + mm(line_ref[piece, :, dh:], s.astype(BF16))
             s = jnp.where(passed, new, s)
         s = mm(before_ref[d, :, dh:], s.astype(BF16)) + before_ref[d, :, :dh].astype(F32)
         state_ref[d * dh:(d + 1) * dh, :] = s.astype(BF16)
@@ -244,34 +248,40 @@
         mixed_ref[here_rows, :] = (joined * lax.rsqrt(mean + EPS) * gain * gate).astype(BF16)
 
 
-def mix_heads(where, before, own, others, local, reach, gate, gain):
+def mix_heads(where, before, others, local, reach, gate, gain):
     vm = pl.BlockSpec(memory_space=pltpu.VMEM)
     dh = local.shape[1]
     return pl.pallas_call(
         mix_kernel,
         out_shape=jax.ShapeDtypeStruct(local.shape, BF16),
-        in_specs=[pl.BlockSpec(memory_space=pltpu.SMEM)] + [vm] * 9,
+        in_specs=[pl.BlockSpec(memory_space=pltpu.SMEM)] + [vm] * 8,
         out_specs=vm,
-        scratch_shapes=[pltpu.VMEM((4,) + own.shape, BF16), pltpu.VMEM((2 * dh, dh), BF16)],
+        scratch_shapes=[pltpu.VMEM((4,) + others[0].shape, BF16), pltpu.VMEM((2 * dh, dh), BF16)],
         name="mix_heads",
-    )(where, before, own, *others, local, reach, gate, gain)
-
-
-def project_kernel(own_ref, one_ref, two_ref, three_ref, w_ref, o0, o1, o2, o3):
+    )(where, before, *others, local, reach, gate, gain)
+
+
+def project_kernel(where_ref, own_ref, one_ref, two_ref, three_ref, w0, w1, w2, w3, o0, o1, o2, o3, line_ref):
     rows = own_ref.shape[0]
+    here = where_ref[1]
     stacked = jnp.concatenate([own_ref[...], one_ref[...], two_ref[...], three_ref[...]], axis=0)
-    parts = mm(stacked, w_ref[...]).astype(BF16)
+    for distance, ref in enumerate((w0, w1, w2, w3)):
+        line_ref[lax.rem(here + 4 - distance, 4)] = mm(stacked, ref[...]).astype(BF16)
     for i, ref in enumerate((o0, o1, o2, o3)):
-        ref[...] = parts[i * rows:(i + 1) * rows]
-
-
-def project(blocks, weight):
-    vm = pl.BlockSpec(memory_space=pltpu.VMEM)
-    shape = jax.ShapeDtypeStruct((blocks[0].shape[0], weight.shape[1]), BF16)
-    return pl.pallas_call(
-        project_kernel, out_shape=(shape,) * 4, in_specs=[vm] * 5, out_specs=(vm,) * 4,
+        ref[...] = jnp.concatenate([line_ref[j, i * rows:(i + 1) * rows, :] for j in range(4)], axis=1)
+
+
+def project(where, blocks, weights):
+    vm = pl.BlockSpec(memory_space=pltpu.VMEM)
+    rows = blocks[0].shape[0]
+    part = weights[0].shape[1]
+    shape = jax.ShapeDtypeStruct((rows, 4 * part), BF16)
+    return pl.pallas_call(
+        project_kernel, out_shape=(shape,) * 4,
+        in_specs=[pl.BlockSpec(memory_space=pltpu.SMEM)] + [vm] * 8, out_specs=(vm,) * 4,
+        scratch_shapes=[pltpu.VMEM((4, 4 * rows, part), BF16)],
         name="project",
-    )(*blocks, weight)
+    )(where, *blocks, *weights)
 
 
 def route_kernel(where_ref, p0, p1, p2, p3, tokens_ref, gain_ref, slots_ref, residual_ref, outgoing_ref, line_ref):
@@ -304,39 +314,72 @@
     )(where, *parts, tokens, gain, slots)
 
 
-def expert_kernel(rows_ref, w_ref, out_ref, sum_ref):
-    j = pl.program_id(0)
-
-    @pl.when(j == 0)
-    def _():
-        sum_ref[...] = jnp.zeros_like(sum_ref)
-
-    width = w_ref.shape[3]
-    both = mm(rows_ref[...], jnp.concatenate([w_ref[0, 0], w_ref[0, 1]], axis=1))
-    gate = both[:, :width]
-    hidden = (gate / (1.0 + jnp.exp(-gate)) * both[:, width:]).astype(BF16)
-    sum_ref[...] += mm_nt(hidden, w_ref[0, 2])
-
-    @pl.when(j == pl.num_programs(0) - 1)
-    def _():
-        out_ref[...] = sum_ref[...].astype(BF16)
+def expert_kernel(rows_ref, w_hbm, out_ref, sum_ref, w_ref, sem):
+    count, _, _, part = w_hbm.shape
+    pair = 2
+
+    def fetch(i):
+        return pltpu.make_async_copy(w_hbm.at[i], w_ref.at[i], sem.at[i])
+
+    for i in range(count):
+        fetch(i).start()
+    sum_ref[...] = jnp.zeros_like(sum_ref)
+    rows = rows_ref[...]
+
+    def step(s, carry):
+        slices = [s * pair + i for i in range(pair)]
+        for i in slices:
+            fetch(i).wait()
+        both = mm(rows, jnp.concatenate([w_ref[i, 0] for i in slices] + [w_ref[i, 1] for i in slices], axis=1))
+        gate = both[:, :pair * part]
+        hidden = (gate / (1.0 + jnp.exp(-gate)) * both[:, pair * part:]).astype(BF16)
+        sum_ref[...] += mm_nt(hidden, jnp.concatenate([w_ref[i, 2] for i in slices], axis=1))
+        return carry
+
+    lax.fori_loop(0, count // pair, step, 0)
+    out_ref[...] = sum_ref[...].astype(BF16)
 
 
 def run_expert(rows, weights):
-    count, _, width, part = weights.shape
+    vm = pl.BlockSpec(memory_space=pltpu.VMEM)
     return pl.pallas_call(
         expert_kernel,
         out_shape=jax.ShapeDtypeStruct(rows.shape, BF16),
-        grid=(count,),
-        in_specs=[
-            pl.BlockSpec(rows.shape, lambda j: (0, 0)),
-            pl.BlockSpec((1, 3, width, part), lambda j: (j, 0, 0, 0)),
+        in_specs=[vm, pl.BlockSpec(memory_space=pl.ANY)],
+        out_specs=vm,
+        scratch_shapes=[
+            pltpu.VMEM(rows.shape, F32),
+            pltpu.VMEM(weights.shape, BF16),
+            pltpu.SemaphoreType.DMA((weights.shape[0],)),
         ],
-        out_specs=pl.BlockSpec(rows.shape, lambda j: (0, 0)),
-        scratch_shapes=[pltpu.VMEM(rows.shape, F32)],
-        compiler_params=pltpu.CompilerParams(dimension_semantics=("arbitrary",)),
         name="run_expert",
     )(rows, weights)
+
+
+def pack_kernel(a_ref, b_ref, c_ref, out_ref, held_ref, in_sem, out_sem):
+    refs = (a_ref, b_ref, c_ref)
+    inward = [pltpu.make_async_copy(ref.at[0], held_ref.at[i], in_sem.at[i]) for i, ref in enumerate(refs)]
+    outward = [pltpu.make_async_copy(held_ref.at[i], out_ref.at[i], out_sem.at[i]) for i in range(3)]
+    for copy in inward:
+        copy.start()
+    for one, other in zip(inward, outward):
+        one.wait()
+        other.start()
+    for copy in outward:
+        copy.wait()
+
+
+def pack(a, b, c):
+    anywhere = pl.BlockSpec(memory_space=pl.ANY)
+    shape = (3,) + a.shape[1:]
+    return pl.pallas_call(
+        pack_kernel,
+        out_shape=jax.ShapeDtypeStruct(shape, BF16),
+        in_specs=[anywhere] * 3,
+        out_specs=anywhere,
+        scratch_shapes=[pltpu.VMEM(shape, BF16), pltpu.SemaphoreType.DMA((3,)), pltpu.SemaphoreType.DMA((3,))],
+        name="pack",
+    )(a, b, c)
 
 
 def finish_kernel(residual_ref, rows_ref, slots_ref, weight_ref, out_ref):
@@ -363,9 +406,13 @@
     )(residual, rows, slots, weight)
 
 
+def shifted(xs, axis):
+    size = lax.axis_size(axis)
+    return [lax.ppermute(x, axis, [(i, (i + d) % size) for i in range(size)]) for d, x in enumerate(xs, 1)]
+
+
 def around(x, axis):
-    size = lax.axis_size(axis)
-    return [lax.ppermute(x, axis, [(i, (i + d) % size) for i in range(size)]) for d in range(1, size)]
+    return shifted([x] * (lax.axis_size(axis) - 1), axis)
 
 
 def shards(
@@ -377,15 +424,9 @@
     chunks = length // CHUNK
     at_x = lax.axis_index("sp_1")
     at_y = lax.axis_index("sp_0")
-    where_x = at_x.astype(jnp.int32).reshape(1)
-    where_y = at_y.astype(jnp.int32).reshape(1)
-
-    quarter = w_out.shape[1] // lax.axis_size("sp_1")
-    w_part = lax.dynamic_slice_in_dim(w_out, at_x * quarter, quarter, 1)
-    w_columns = lax.all_gather(w_part, "tp", axis=0, tiled=True)
-    experts = jnp.concatenate([expert_gate, expert_up, expert_down], axis=0)
-    experts, w_columns = lax.optimization_barrier((experts, w_columns)) if False else (experts, w_columns)
-    expert_all = lax.all_gather(experts, "tp", axis=0)
+    where = jnp.stack([at_x, at_y]).astype(jnp.int32)
+
+    expert_all = lax.all_gather(pack(expert_gate, expert_up, expert_down), "tp", axis=0)
 
     local_rows = tokens.shape[0]
     group_count = group_logits.shape[1]
@@ -420,19 +461,25 @@
         decay_pre.reshape(2 * chunks, CHUNK), decay_shock.reshape(2 * chunks, CHUNK),
         beta_pre.reshape(2 * chunks, CHUNK),
     )
-    before, line = compose_line(where_x, maps, around(maps, "sp_1"))
+    sixteenth = w_out.shape[1] // lax.axis_size(SP)
+    w_out, maps = lax.optimization_barrier((w_out, maps))
+    w_part = lax.dynamic_slice_in_dim(w_out, (at_x * lax.axis_size("sp_0") + at_y) * sixteenth, sixteenth, 1)
+    w_column = lax.all_gather(w_part, "tp", axis=0, tiled=True)
+    before, *sends = compose_line(where, maps, around(maps, "sp_1"))
     mixed = mix_heads(
-        where_y, before, line, around(line, "sp_0"), local, reach,
+        where, before, shifted(sends, "sp_0"), local, reach,
         out_gate.reshape(length, dh), head_gain.reshape(1, dh),
     )
+    mixed, w_column = lax.optimization_barrier((mixed, w_column))
+    w_columns = [w_column] + around(w_column, "sp_0")
     mine = lax.all_to_all(mixed, "tp", split_axis=0, concat_axis=1, tiled=True)
-    parts = project([mine] + around(mine, "sp_1"), w_columns)
+    parts = project(where, [mine] + around(mine, "sp_1"), w_columns)
     size = lax.axis_size("sp_1")
     returned = [parts[0]] + [
         lax.ppermute(parts[d], "sp_1", [(i, (i - d) % size) for i in range(size)]) for d in range(1, size)
     ]
     residual, outgoing = route(
-        where_x, returned, tokens, norm_gain.reshape(1, -1), slot_place.T, expert_count * capacity
+        where, returned, tokens, norm_gain.reshape(1, -1), slot_place.T, expert_count * capacity
     )
     width = outgoing.shape[1]
     outgoing = outgoing.reshape(expert_count, capacity, width)

time: 242 us -> 196 us (0.81)
  waiting for transfers between devices: 127 us -> 66.2 us
  blocking collectives: 0 us -> 26.9 us
  Pallas kernels: 48.9 us -> 42.6 us
  starting transfers between devices: 39.9 us -> 34.7 us
    all_gather x2 -> x1, waiting for transfers between devices: 68.8 us -> 17.1 us  [shards(): lax.all_gather(pack(expert_gate, expert_up, expert_down), 'tp', axis=0)]
    all_gather x0 -> x1, blocking collectives: none -> 26.9 us  [shards(): w_column = lax.all_gather(w_part, 'tp', axis=0, tiled=True)]
    pallas_call x1, Pallas kernels: 20.2 us -> 11.1 us  [run_expert(): pl.pallas_call(expert_kernel, out_shape=jax.ShapeDtypeStruct(rows.shape,...]
    all_to_all x1, starting transfers between devices: 10.8 us -> 3.86 us  [shards(): mine = lax.all_to_all(mixed, 'tp', split_axis=0, concat_axis=1, tiled=True)]
    all_to_all x1, waiting for transfers between devices: 14.3 us -> 11.1 us  [shards(): mine = lax.all_to_all(mixed, 'tp', split_axis=0, concat_axis=1, tiled=True)]
    pallas_call x1 -> x2, Pallas kernels: 3.38 us -> 6.25 us  [the longest x1 3.94 us: project(): pl.pallas_call(project_kernel, out_shape=(shape,) * 4, in_specs=[pl.Block...]
    ppermute x9 -> x12, waiting for transfers between devices: 20.1 us -> 17.3 us  [shifted(): lax.ppermute(x, axis, [(i, (i + d) % size) for i in range(size)])]
    concatenate x1 -> x0, other arithmetic: 2.67 us -> none  [shards(): experts = jnp.concatenate([expert_gate, expert_up, expert_down], axis=0)]
  transfers between devices with their start and end apart: 17 -> 19, of which waited for: 15 -> 11; matrix products, arithmetic and copies ran while one was open for 2% -> 4% of each run, Pallas kernels for 11% -> 14%
where the time goes in v2:
time: 196 us; the launch traced here: 195 us
  waiting for transfers between devices  66.2 us (34%)
  Pallas kernels  42.6 us (22%)
  starting transfers between devices  34.7 us (18%)
  blocking collectives  26.9 us (14%)
  between operations  13.6 us (7%)
  local copies, waits for them, and re-layouts  5.52 us (3%)
  other arithmetic  5.44 us (3%)
    all_gather x1, blocking collectives, shards(): w_column = lax.all_gather(w_part, 'tp', axis=0, tiled=True)  26.9 us
    ppermute x12, starting transfers between devices, shifted(): lax.ppermute(x, axis, [(i, (i + d) % size) for i in range(size)])  17.5 us
    ppermute x12, waiting for transfers between devices, shifted(): lax.ppermute(x, axis, [(i, (i + d) % size) for i in range(size)])  17.3 us
    all_gather x1, waiting for transfers between devices, shards(): lax.all_gather(pack(expert_gate, expert_up, expert_down), 'tp', axis=0)  17.1 us
    pallas_call x1, Pallas kernels, local_attention(): pl.pallas_call(local_kernel, out_shape=(jax.ShapeDtypeStruct((length, dh)...  14.9 us
    pallas_call x1, Pallas kernels, run_expert(): pl.pallas_call(expert_kernel, out_shape=jax.ShapeDtypeStruct(rows.shape,...  11.1 us
    all_to_all x1, waiting for transfers between devices, shards(): mine = lax.all_to_all(mixed, 'tp', split_axis=0, concat_axis=1, tiled=True)  11.1 us
    all_to_all x1, waiting for transfers between devices, shards(): lax.all_to_all(expert_rows, SP, split_axis=0, concat_axis=0, tiled=True)  9.27 us
  transfers between devices with their start and end apart: 19, of which 11 were waited for; matrix products, arithmetic and copies ran while one was open for 4% of the time, Pallas kernels for 14%

profile of v2, /device:TPU:1, one launch (start us, length us, event | category | flops | bytes accessed | tf_op | source)
XLA Modules:
  0.0 195.1 jit_solution(16735910119532150492)
XLA Ops:
  6.5 2.3 %pack.1 = bf16[3,2048,128]{2,1,0:T(8,128)(2,1)} custom-call(bf16[1,2048,128]{2,1,0:T(8,128)(2,1)} %a_ref.1, bf16[1,2048,128]{2,1,0:T(8,128)(2,1)} %b_ref.1, bf16[1,2048,128]{2,1,0:T(8,128)(2,1)} %c_ref.1), custom_call_target="tpu_custom_call" | custom-call | tf_op jit(solution)/shard_map/pack/pallas_call | solution.py:375
  8.9 0.0 all-gather.3.cloned.1.call-update
  8.9 1.3 copy.48.rate_ref
  10.2 14.9 %local_attention.1 = (f32[1024,128]{1,0:T(8,128)}, bf16[1024,256]{1,0:T(8,128)(2,1)}, bf16[2,128,256]{2,1,0:T(8,128)(2,1)}) custom-call(f32[2,1]{1,0:T(2,128)} %copy.48.rate_ref, bf16[1024,128]{1,0:T(8,128)(2,1)} %bitcast.33, bf16[1024,128]{1,0:T(8,128)(2,1)} %bitcast.34, bf16[1024,128]{1,0:T(8,128)(2,1)} %bitcast.35, f32[16,128]{1,0:T(8,128)} %bitcast.37, ...), custom_call_target="tpu_custom_call" | custom-call | tf_op jit(solution)/shard_map/local_attention/pallas_call | solution.py:160
  25.0 2.0 %collective-permute-start = (bf16[2,128,256]{2,1,0:T(8,128)(2,1)}, bf16[2,128,256]{2,1,0:T(8,128)(2,1)S(1)}, u32[]{:S(2)}, u32[]{:S(2)}) collective-permute-start(bf16[2,128,256]{2,1,0:T(8,128)(2,1)} %get-tuple-element.23.own_ref), channel_id=1, source_target_pairs={{0,16},{16,32},{32,48},{48,0},{1,17},{17,33},{33,49},{49,1},{2,18}... | collective-permute-start | bytes 393224 | tf_op jit(solution)/shard_map/ppermute | solution.py:411
  27.0 2.5 %collective-permute-start.1 = (bf16[2,128,256]{2,1,0:T(8,128)(2,1)}, bf16[2,128,256]{2,1,0:T(8,128)(2,1)S(1)}, u32[]{:S(2)}, u32[]{:S(2)}) collective-permute-start(bf16[2,128,256]{2,1,0:T(8,128)(2,1)} %get-tuple-element.23.own_ref), channel_id=1, source_target_pairs={{0,32},{16,48},{32,0},{48,16},{1,33},{17,49},{33,1},{49,17},{2,34}... | collective-permute-start | bytes 393224 | tf_op jit(solution)/shard_map/ppermute | solution.py:411
  29.5 1.1 collective-permute-start.2
  30.6 0.7 pad_add_fusion.where_ref
  31.3 0.0 collective-permute-done.one_ref
  31.3 4.1 %collective-permute-done.1.two_ref = bf16[2,128,256]{2,1,0:T(8,128)(2,1)S(1)} collective-permute-done((bf16[2,128,256]{2,1,0:T(8,128)(2,1)}, bf16[2,128,256]{2,1,0:T(8,128)(2,1)S(1)}, u32[]{:S(2)}, u32[]{:S(2)}) %collective-permute-start.1) | collective-permute-done | bytes 131104 | tf_op jit(solution)/shard_map/ppermute | solution.py:411
  35.4 0.0 collective-permute-done.2.three_ref
  35.4 0.6 copy-done.11
  36.1 0.7 copy-done.12
  36.7 2.5 %compose_line.1 = (bf16[2,128,256]{2,1,0:T(8,128)(2,1)}, bf16[128,256]{1,0:T(8,128)(2,1)}, bf16[128,256]{1,0:T(8,128)(2,1)}, bf16[128,256]{1,0:T(8,128)(2,1)}) custom-call(s32[2]{0:T(128)} %pad_add_fusion.where_ref, bf16[2,128,256]{2,1,0:T(8,128)(2,1)} %get-tuple-element.23.own_ref, bf16[2,128,256]{2,1,0:T(8,128)(2,1)} %copy-done.10, ...), custom_call_target="tpu_custom_call" | custom-call | tf_op jit(solution)/shard_map/compose_line/pallas_call | solution.py:211
  39.2 1.3 collective-permute-start.3
  40.5 2.6 %collective-permute-start.4 = (bf16[128,256]{1,0:T(8,128)(2,1)}, bf16[128,256]{1,0:T(8,128)(2,1)S(1)}, u32[]{:S(2)}, u32[]{:S(2)}) collective-permute-start(bf16[128,256]{1,0:T(8,128)(2,1)} %get-tuple-element.26), channel_id=1, source_target_pairs={{0,128},{64,192},{128,0},{192,64},{1,129},{65,193},{129,1},{193,65... | collective-permute-start | bytes 196616 | tf_op jit(solution)/shard_map/ppermute | solution.py:411
  43.1 1.1 collective-permute-start.5
  44.2 26.9 %all_gather.9.w0 = bf16[2048,128]{1,0:T(8,128)(2,1)S(1)} all-gather(bf16[128,128]{1,0:T(8,128)(2,1)S(1)} %constant_dynamic-slice_fusion), channel_id=1, replica_groups=mesh['sp_0'=4,'sp_1'=4,'tp'=16] {'tp'}, dimensions={0}, use_global_device_ids=true | all-gather | bytes 557056 | tf_op jit(solution)/shard_map/all_gather | solution.py:467
  71.1 0.0 collective-permute-done.3.one_ref
  71.1 0.0 collective-permute-done.4.two_ref
  71.1 0.0 collective-permute-done.5.three_ref
  71.1 0.6 copy-done.13
  71.7 0.0 copy-done.15
  71.8 0.0 copy-done.17
  71.8 3.2 %mix_heads.1 = bf16[1024,128]{1,0:T(8,128)(2,1)} custom-call(s32[2]{0:T(128)} %pad_add_fusion.where_ref, bf16[2,128,256]{2,1,0:T(8,128)(2,1)} %get-tuple-element.24.before_ref, bf16[128,256]{1,0:T(8,128)(2,1)} %copy-done.13, bf16[128,256]{1,0:T(8,128)(2,1)} %copy-done.15, bf16[128,256]{1,0:T(8,128)(2,1)} %copy-done.17, ...), custom_call_target="tpu_custom_call" | custom-call | tf_op jit(solution)/shard_map/mix_heads/pallas_call | solution.py:254
  75.0 3.9 %all-to-all-start = ((bf16[16,64,128]{2,1,0:T(8,128)(2,1)}), bf16[16,64,128]{2,1,0:T(8,128)(2,1)S(1)}, u32[]{:S(2)}, u32[]{:S(2)}) async-start(bf16[16,64,128]{2,1,0:T(8,128)(2,1)} %bitcast.30), calls=%async_computation | async-start | bytes 524288 | tf_op jit(solution)/shard_map/all_to_all | solution.py:475
  78.8 0.4 collective-permute-start.9
  79.2 0.7 convert_reduce_fusion
  79.9 0.6 collective-permute-start.10
  80.5 1.8 collective-permute-start.11
  82.3 11.1 %all-to-all-done = bf16[16,64,128]{2,1,0:T(8,128)(2,1)S(1)} async-done(((bf16[16,64,128]{2,1,0:T(8,128)(2,1)}), bf16[16,64,128]{2,1,0:T(8,128)(2,1)S(1)}, u32[]{:S(2)}, u32[]{:S(2)}) %all-to-all-start) | async-done | bytes 262176 | tf_op jit(solution)/shard_map/all_to_all | solution.py:475
  93.4 0.0 copy-start.4
  93.5 0.6 collective-permute-start.6
  94.0 2.2 %collective-permute-start.7 = (bf16[64,2048]{1,0:T(8,128)(2,1)S(1)}, bf16[64,2048]{1,0:T(8,128)(2,1)S(1)}, u32[]{:S(2)}, u32[]{:S(2)}) collective-permute-start(bf16[64,2048]{1,0:T(8,128)(2,1)S(1)} %copy_bitcast_fusion.own_ref), channel_id=1, source_target_pairs={{0,32},{16,48},{32,0},{48,16},{1,33},{17,49},{33,1},{49,17},{2,34}... | collective-permute-start | bytes 786440 | tf_op jit(solution)/shard_map/ppermute | solution.py:411
  96.2 8.4 %collective-permute-done.9.w1 = bf16[2048,128]{1,0:T(8,128)(2,1)S(1)} collective-permute-done((bf16[2048,128]{1,0:T(8,128)(2,1)S(1)}, bf16[2048,128]{1,0:T(8,128)(2,1)S(1)}, u32[]{:S(2)}, u32[]{:S(2)}) %collective-permute-start.9) | collective-permute-done | bytes 524320 | tf_op jit(solution)/shard_map/ppermute | solution.py:411
  104.7 1.4 collective-permute-start.8
  106.0 0.1 convolution_convert_fusion
  106.2 0.7 select_reduce_fusion
  106.9 0.0 collective-permute-done.10.w2
  106.9 0.0 collective-permute-done.11.w3
  106.9 1.4 collective-permute-done.7.two_ref
  108.3 3.4 %collective-permute-done.8.three_ref = bf16[64,2048]{1,0:T(8,128)(2,1)} collective-permute-done((bf16[64,2048]{1,0:T(8,128)(2,1)S(1)}, bf16[64,2048]{1,0:T(8,128)(2,1)}, u32[]{:S(2)}, u32[]{:S(2)}) %collective-permute-start.8) | collective-permute-done | bytes 262176 | tf_op jit(solution)/shard_map/ppermute | solution.py:411
  111.8 3.9 %project.1 = (bf16[64,512]{1,0:T(8,128)(2,1)}, bf16[64,512]{1,0:T(8,128)(2,1)}, bf16[64,512]{1,0:T(8,128)(2,1)}, bf16[64,512]{1,0:T(8,128)(2,1)}) custom-call(s32[2]{0:T(128)} %pad_add_fusion.where_ref, bf16[64,2048]{1,0:T(8,128)(2,1)} %copy-done.4, bf16[64,2048]{1,0:T(8,128)(2,1)} %copy-done.8, bf16[64,2048]{1,0:T(8,128)(2,1)} %copy-done.9, ...), custom_call_target="tpu_custom_call" | custom-call | tf_op jit(solution)/shard_map/project/pallas_call | solution.py:279
  115.7 2.6 %collective-permute-start.12 = (bf16[64,512]{1,0:T(8,128)(2,1)}, bf16[64,512]{1,0:T(8,128)(2,1)S(1)}, u32[]{:S(2)}, u32[]{:S(2)}) collective-permute-start(bf16[64,512]{1,0:T(8,128)(2,1)} %get-tuple-element.34), channel_id=1, source_target_pairs={{0,48},{16,0},{32,16},{48,32},{1,49},{17,1},{33,17},{49,33},{2,50}... | collective-permute-start | bytes 196616 | tf_op jit(solution)/shard_map/ppermute | solution.py:479
  118.3 0.7 collective-permute-start.14
  118.9 1.3 multiply_add_fusion
  120.2 0.3 collective-permute-done.12.p1
  120.5 2.7 %collective-permute-done.13.p2 = bf16[64,512]{1,0:T(8,128)(2,1)S(1)} collective-permute-done((bf16[64,512]{1,0:T(8,128)(2,1)}, bf16[64,512]{1,0:T(8,128)(2,1)S(1)}, u32[]{:S(2)}, u32[]{:S(2)}) %collective-permute-start.13) | collective-permute-done | bytes 65568 | tf_op jit(solution)/shard_map/ppermute | solution.py:479
  123.2 0.7 collective-permute-done.14.p3
  123.9 0.6 copy-done.18
  124.5 2.4 %route.1 = (f32[64,2048]{1,0:T(8,128)}, bf16[128,2048]{1,0:T(8,128)(2,1)}) custom-call(s32[2]{0:T(128)} %pad_add_fusion.where_ref, bf16[64,512]{1,0:T(8,128)(2,1)} %get-tuple-element.33.p0, bf16[64,512]{1,0:T(8,128)(2,1)} %copy-done.14, bf16[64,512]{1,0:T(8,128)(2,1)} %copy-done.16, bf16[64,512]{1,0:T(8,128)(2,1)} %copy-done.18, ...), custom_call_target="tpu_custom_call" | custom-call | tf_op jit(solution)/shard_map/route/pallas_call | solution.py:304
  126.9 3.6 %all-to-all-start.1 = ((bf16[16,8,2048]{2,1,0:T(8,128)(2,1)}), bf16[16,8,2048]{2,1,0:T(8,128)(2,1)S(1)}, u32[]{:S(2)}, u32[]{:S(2)}) async-start(bf16[16,8,2048]{2,1,0:T(8,128)(2,1)} %bitcast.31), calls=%async_computation.1 | async-start | bytes 1048576 | tf_op jit(solution)/shard_map/all_to_all | solution.py:486
  130.5 0.7 exponential_reduce_fusion.1
  131.2 0.7 exponential_divide_fusion
  131.9 7.7 %all-to-all-done.1 = bf16[16,8,2048]{2,1,0:T(8,128)(2,1)S(1)} async-done(((bf16[16,8,2048]{2,1,0:T(8,128)(2,1)}), bf16[16,8,2048]{2,1,0:T(8,128)(2,1)S(1)}, u32[]{:S(2)}, u32[]{:S(2)}) %all-to-all-start.1) | async-done | bytes 524320 | tf_op jit(solution)/shard_map/all_to_all | solution.py:486
  139.6 17.1 %all-gather.3.cloned.1.call-done = bf16[48,2048,128]{2,1,0:T(8,128)(2,1)} async-done(((bf16[3,2048,128]{2,1,0:T(8,128)(2,1)}), bf16[48,2048,128]{2,1,0:T(8,128)(2,1)}) %all-gather.3.cloned.1.call-update) | async-done | bytes 25165840 | tf_op jit(solution)/shard_map/all_gather | solution.py:429
  156.7 11.1 %run_expert.1 = bf16[128,2048]{1,0:T(8,128)(2,1)} custom-call(bf16[128,2048]{1,0:T(8,128)(2,1)} %bitcast.28, bf16[16,3,2048,128]{3,2,1,0:T(8,128)(2,1)} %bitcast.26), custom_call_target="tpu_custom_call" | custom-call | tf_op jit(solution)/shard_map/run_expert/pallas_call | solution.py:345
  167.8 6.6 %all-to-all-start.2 = ((bf16[16,8,2048]{2,1,0:T(8,128)(2,1)}), bf16[16,8,2048]{2,1,0:T(8,128)(2,1)S(1)}, u32[]{:S(2)}, u32[]{:S(2)}) async-start(bf16[16,8,2048]{2,1,0:T(8,128)(2,1)} %bitcast.27), calls=%async_computation.2 | async-start | bytes 1048576 | tf_op jit(solution)/shard_map/all_to_all | solution.py:489
  174.4 0.7 copy.53.slots_ref
  175.1 0.1 copy.51
  175.3 0.7 broadcast_multiply_fusion.weight_ref
  176.0 9.3 %all-to-all-done.2 = bf16[16,8,2048]{2,1,0:T(8,128)(2,1)S(1)} async-done(((bf16[16,8,2048]{2,1,0:T(8,128)(2,1)}), bf16[16,8,2048]{2,1,0:T(8,128)(2,1)S(1)}, u32[]{:S(2)}, u32[]{:S(2)}) %all-to-all-start.2) | async-done | bytes 524320 | tf_op jit(solution)/shard_map/all_to_all | solution.py:489
  185.2 0.8 copy-done.2
  186.0 2.3 %finish.1 = bf16[64,2048]{1,0:T(8,128)(2,1)} custom-call(f32[64,2048]{1,0:T(8,128)} %get-tuple-element.37.residual_ref, bf16[128,2048]{1,0:T(8,128)(2,1)} %bitcast.29, s32[64,2]{1,0:T(8,128)} %copy.53.slots_ref, f32[64,2]{1,0:T(8,128)} %broadcast_multiply_fusion.weight_ref), custom_call_target="tpu_custom_call" | custom-call | tf_op jit(solution)/shard_map/finish/pallas_call | solution.py:400
  (44 shorter events, 0.2 us)
Async XLA Ops:
  6.5 24.8 %copy-start = (bf16[128,2048]{1,0:T(8,128)(2,1)S(1)}, bf16[128,2048]{1,0:T(8,128)(2,1)}, u32[]{:S(2)}) copy-start(bf16[128,2048]{1,0:T(8,128)(2,1)} %param.27) | copy-start | bytes 1572868
  6.5 167.9 %copy-start.21 = (s32[64,2]{0,1:T(2,128)S(1)}, s32[64,2]{0,1:T(2,128)}, u32[]{:S(2)}) copy-start(s32[64,2]{0,1:T(2,128)} %param.30) | copy-start | bytes 1540
  6.5 168.7 %copy-start.19 = (f32[64,8]{0,1:T(8,128)S(1)}, f32[64,8]{0,1:T(8,128)}, u32[]{:S(2)}) copy-start(f32[64,8]{0,1:T(8,128)} %param.32) | copy-start | bytes 6148
  6.5 150.1 %all-gather.3.cloned.1.call-start = ((), (), s32[]{:S(2)}) async-start(), calls=%async_computation.3 | async-start | bytes 26738688 | tf_op jit(solution)/shard_map/all_gather | solution.py:429
  25.0 6.3 %collective-permute-start = (bf16[2,128,256]{2,1,0:T(8,128)(2,1)}, bf16[2,128,256]{2,1,0:T(8,128)(2,1)S(1)}, u32[]{:S(2)}, u32[]{:S(2)}) collective-permute-start(bf16[2,128,256]{2,1,0:T(8,128)(2,1)} %get-tuple-element.23.own_ref), channel_id=1, source_target_pairs={{0,16},{16,32},{32,48},{48,0},{1,17},{17,33},{33,49},{49,1},{2,18}... | collective-permute-start | bytes 393224 | tf_op jit(solution)/shard_map/ppermute | solution.py:411
  27.0 8.4 %collective-permute-start.1 = (bf16[2,128,256]{2,1,0:T(8,128)(2,1)}, bf16[2,128,256]{2,1,0:T(8,128)(2,1)S(1)}, u32[]{:S(2)}, u32[]{:S(2)}) collective-permute-start(bf16[2,128,256]{2,1,0:T(8,128)(2,1)} %get-tuple-element.23.own_ref), channel_id=1, source_target_pairs={{0,32},{16,48},{32,0},{48,16},{1,33},{17,49},{33,1},{49,17},{2,34}... | collective-permute-start | bytes 393224 | tf_op jit(solution)/shard_map/ppermute | solution.py:411
  29.5 5.9 %collective-permute-start.2 = (bf16[2,128,256]{2,1,0:T(8,128)(2,1)}, bf16[2,128,256]{2,1,0:T(8,128)(2,1)S(1)}, u32[]{:S(2)}, u32[]{:S(2)}) collective-permute-start(bf16[2,128,256]{2,1,0:T(8,128)(2,1)} %get-tuple-element.23.own_ref), channel_id=1, source_target_pairs={{0,48},{16,0},{32,16},{48,32},{1,49},{17,1},{33,17},{49,33},{2,50}... | collective-permute-start | bytes 393224 | tf_op jit(solution)/shard_map/ppermute | solution.py:411
  31.3 4.1 %copy-start.10 = (bf16[2,128,256]{2,1,0:T(8,128)(2,1)}, bf16[2,128,256]{2,1,0:T(8,128)(2,1)S(1)}, u32[]{:S(2)}) copy-start(bf16[2,128,256]{2,1,0:T(8,128)(2,1)S(1)} %collective-permute-done.one_ref) | copy-start | bytes 393220
  35.4 0.6 copy-start.11
  36.1 0.7 copy-start.12
  39.2 31.8 %collective-permute-start.3 = (bf16[128,256]{1,0:T(8,128)(2,1)}, bf16[128,256]{1,0:T(8,128)(2,1)S(1)}, u32[]{:S(2)}, u32[]{:S(2)}) collective-permute-start(bf16[128,256]{1,0:T(8,128)(2,1)} %get-tuple-element.25), channel_id=1, source_target_pairs={{0,64},{64,128},{128,192},{192,0},{1,65},{65,129},{129,193},{193,1... | collective-permute-start | bytes 196616 | tf_op jit(solution)/shard_map/ppermute | solution.py:411
  40.5 30.6 %collective-permute-start.4 = (bf16[128,256]{1,0:T(8,128)(2,1)}, bf16[128,256]{1,0:T(8,128)(2,1)S(1)}, u32[]{:S(2)}, u32[]{:S(2)}) collective-permute-start(bf16[128,256]{1,0:T(8,128)(2,1)} %get-tuple-element.26), channel_id=1, source_target_pairs={{0,128},{64,192},{128,0},{192,64},{1,129},{65,193},{129,1},{193,65... | collective-permute-start | bytes 196616 | tf_op jit(solution)/shard_map/ppermute | solution.py:411
  43.1 28.0 %collective-permute-start.5 = (bf16[128,256]{1,0:T(8,128)(2,1)}, bf16[128,256]{1,0:T(8,128)(2,1)S(1)}, u32[]{:S(2)}, u32[]{:S(2)}) collective-permute-start(bf16[128,256]{1,0:T(8,128)(2,1)} %get-tuple-element.27), channel_id=1, source_target_pairs={{0,192},{64,0},{128,64},{192,128},{1,193},{65,1},{129,65},{193,129... | collective-permute-start | bytes 196616 | tf_op jit(solution)/shard_map/ppermute | solution.py:411
  71.1 40.6 %copy-start.3 = (bf16[2048,128]{1,0:T(8,128)(2,1)}, bf16[2048,128]{1,0:T(8,128)(2,1)S(1)}, u32[]{:S(2)}) copy-start(bf16[2048,128]{1,0:T(8,128)(2,1)S(1)} %all_gather.9.w0) | copy-start | bytes 1572868
  71.1 0.6 copy-start.13
  71.1 0.7 copy-start.15
  71.1 0.7 copy-start.17
  75.0 18.4 %all-to-all-start = ((bf16[16,64,128]{2,1,0:T(8,128)(2,1)}), bf16[16,64,128]{2,1,0:T(8,128)(2,1)S(1)}, u32[]{:S(2)}, u32[]{:S(2)}) async-start(bf16[16,64,128]{2,1,0:T(8,128)(2,1)} %bitcast.30), calls=%async_computation | async-start | bytes 524288 | tf_op jit(solution)/shard_map/all_to_all | solution.py:475
  78.8 25.9 %collective-permute-start.9 = (bf16[2048,128]{1,0:T(8,128)(2,1)S(1)}, bf16[2048,128]{1,0:T(8,128)(2,1)S(1)}, u32[]{:S(2)}, u32[]{:S(2)}) collective-permute-start(bf16[2048,128]{1,0:T(8,128)(2,1)S(1)} %all_gather.9.w0), channel_id=1, source_target_pairs={{0,64},{64,128},{128,192},{192,0},{1,65},{65,129},{129,193},{193,1... | collective-permute-start | bytes 1572872 | tf_op jit(solution)/shard_map/ppermute | solution.py:411
  79.9 27.0 %collective-permute-start.10 = (bf16[2048,128]{1,0:T(8,128)(2,1)S(1)}, bf16[2048,128]{1,0:T(8,128)(2,1)S(1)}, u32[]{:S(2)}, u32[]{:S(2)}) collective-permute-start(bf16[2048,128]{1,0:T(8,128)(2,1)S(1)} %all_gather.9.w0), channel_id=1, source_target_pairs={{0,128},{64,192},{128,0},{192,64},{1,129},{65,193},{129,1},{193,65... | collective-permute-start | bytes 1572872 | tf_op jit(solution)/shard_map/ppermute | solution.py:411
  80.5 26.4 %collective-permute-start.11 = (bf16[2048,128]{1,0:T(8,128)(2,1)S(1)}, bf16[2048,128]{1,0:T(8,128)(2,1)S(1)}, u32[]{:S(2)}, u32[]{:S(2)}) collective-permute-start(bf16[2048,128]{1,0:T(8,128)(2,1)S(1)} %all_gather.9.w0), channel_id=1, source_target_pairs={{0,192},{64,0},{128,64},{192,128},{1,193},{65,1},{129,65},{193,129... | collective-permute-start | bytes 1572872 | tf_op jit(solution)/shard_map/ppermute | solution.py:411
  93.4 18.3 %copy-start.4 = (bf16[64,2048]{1,0:T(8,128)(2,1)}, bf16[64,2048]{1,0:T(8,128)(2,1)S(1)}, u32[]{:S(2)}) copy-start(bf16[64,2048]{1,0:T(8,128)(2,1)S(1)} %copy_bitcast_fusion.own_ref) | copy-start | bytes 786436
  93.5 13.5 %collective-permute-start.6 = (bf16[64,2048]{1,0:T(8,128)(2,1)S(1)}, bf16[64,2048]{1,0:T(8,128)(2,1)S(1)}, u32[]{:S(2)}, u32[]{:S(2)}) collective-permute-start(bf16[64,2048]{1,0:T(8,128)(2,1)S(1)} %copy_bitcast_fusion.own_ref), channel_id=1, source_target_pairs={{0,16},{16,32},{32,48},{48,0},{1,17},{17,33},{33,49},{49,1},{2,18}... | collective-permute-start | bytes 786440 | tf_op jit(solution)/shard_map/ppermute | solution.py:411
  94.0 14.3 %collective-permute-start.7 = (bf16[64,2048]{1,0:T(8,128)(2,1)S(1)}, bf16[64,2048]{1,0:T(8,128)(2,1)S(1)}, u32[]{:S(2)}, u32[]{:S(2)}) collective-permute-start(bf16[64,2048]{1,0:T(8,128)(2,1)S(1)} %copy_bitcast_fusion.own_ref), channel_id=1, source_target_pairs={{0,32},{16,48},{32,0},{48,16},{1,33},{17,49},{33,1},{49,17},{2,34}... | collective-permute-start | bytes 786440 | tf_op jit(solution)/shard_map/ppermute | solution.py:411
  104.7 7.0 %copy-start.5 = (bf16[2048,128]{1,0:T(8,128)(2,1)}, bf16[2048,128]{1,0:T(8,128)(2,1)S(1)}, u32[]{:S(2)}) copy-start(bf16[2048,128]{1,0:T(8,128)(2,1)S(1)} %collective-permute-done.9.w1) | copy-start | bytes 1572868
  104.7 7.0 %collective-permute-start.8 = (bf16[64,2048]{1,0:T(8,128)(2,1)S(1)}, bf16[64,2048]{1,0:T(8,128)(2,1)}, u32[]{:S(2)}, u32[]{:S(2)}) collective-permute-start(bf16[64,2048]{1,0:T(8,128)(2,1)S(1)} %copy_bitcast_fusion.own_ref), channel_id=1, source_target_pairs={{0,48},{16,0},{32,16},{48,32},{1,49},{17,1},{33,17},{49,33},{2,50}... | collective-permute-start | bytes 786440 | tf_op jit(solution)/shard_map/ppermute | solution.py:411
  106.9 4.8 %copy-start.6 = (bf16[2048,128]{1,0:T(8,128)(2,1)}, bf16[2048,128]{1,0:T(8,128)(2,1)S(1)}, u32[]{:S(2)}) copy-start(bf16[2048,128]{1,0:T(8,128)(2,1)S(1)} %collective-permute-done.10.w2) | copy-start | bytes 1572868
  106.9 4.8 %copy-start.7 = (bf16[2048,128]{1,0:T(8,128)(2,1)}, bf16[2048,128]{1,0:T(8,128)(2,1)S(1)}, u32[]{:S(2)}) copy-start(bf16[2048,128]{1,0:T(8,128)(2,1)S(1)} %collective-permute-done.11.w3) | copy-start | bytes 1572868
  106.9 4.8 %copy-start.8 = (bf16[64,2048]{1,0:T(8,128)(2,1)}, bf16[64,2048]{1,0:T(8,128)(2,1)S(1)}, u32[]{:S(2)}) copy-start(bf16[64,2048]{1,0:T(8,128)(2,1)S(1)} %collective-permute-done.6.one_ref) | copy-start | bytes 786436
  108.3 3.5 %copy-start.9 = (bf16[64,2048]{1,0:T(8,128)(2,1)}, bf16[64,2048]{1,0:T(8,128)(2,1)S(1)}, u32[]{:S(2)}) copy-start(bf16[64,2048]{1,0:T(8,128)(2,1)S(1)} %collective-permute-done.7.two_ref) | copy-start | bytes 786436
  115.7 4.8 %collective-permute-start.12 = (bf16[64,512]{1,0:T(8,128)(2,1)}, bf16[64,512]{1,0:T(8,128)(2,1)S(1)}, u32[]{:S(2)}, u32[]{:S(2)}) collective-permute-start(bf16[64,512]{1,0:T(8,128)(2,1)} %get-tuple-element.34), channel_id=1, source_target_pairs={{0,48},{16,0},{32,16},{48,32},{1,49},{17,1},{33,17},{49,33},{2,50}... | collective-permute-start | bytes 196616 | tf_op jit(solution)/shard_map/ppermute | solution.py:479
  118.3 4.9 %collective-permute-start.13 = (bf16[64,512]{1,0:T(8,128)(2,1)}, bf16[64,512]{1,0:T(8,128)(2,1)S(1)}, u32[]{:S(2)}, u32[]{:S(2)}) collective-permute-start(bf16[64,512]{1,0:T(8,128)(2,1)} %get-tuple-element.35), channel_id=1, source_target_pairs={{0,32},{16,48},{32,0},{48,16},{1,33},{17,49},{33,1},{49,17},{2,34}... | collective-permute-start | bytes 196616 | tf_op jit(solution)/shard_map/ppermute | solution.py:479
  118.3 5.6 %collective-permute-start.14 = (bf16[64,512]{1,0:T(8,128)(2,1)}, bf16[64,512]{1,0:T(8,128)(2,1)S(1)}, u32[]{:S(2)}, u32[]{:S(2)}) collective-permute-start(bf16[64,512]{1,0:T(8,128)(2,1)} %get-tuple-element.36), channel_id=1, source_target_pairs={{0,16},{16,32},{32,48},{48,0},{1,17},{17,33},{33,49},{49,1},{2,18}... | collective-permute-start | bytes 196616 | tf_op jit(solution)/shard_map/ppermute | solution.py:479
  120.2 54.2 %copy-start.20 = (s32[64,2]{0,1:T(2,128)S(1)}, s32[64,2]{0,1:T(2,128)}, u32[]{:S(2)}) copy-start(s32[64,2]{0,1:T(2,128)} %multiply_add_fusion) | copy-start | bytes 1540
  120.5 3.4 %copy-start.14 = (bf16[64,512]{1,0:T(8,128)(2,1)}, bf16[64,512]{1,0:T(8,128)(2,1)S(1)}, u32[]{:S(2)}) copy-start(bf16[64,512]{1,0:T(8,128)(2,1)S(1)} %collective-permute-done.12.p1) | copy-start | bytes 196612
  123.2 0.7 copy-start.16
  123.9 0.6 copy-start.18
  126.9 12.6 %all-to-all-start.1 = ((bf16[16,8,2048]{2,1,0:T(8,128)(2,1)}), bf16[16,8,2048]{2,1,0:T(8,128)(2,1)S(1)}, u32[]{:S(2)}, u32[]{:S(2)}) async-start(bf16[16,8,2048]{2,1,0:T(8,128)(2,1)} %bitcast.31), calls=%async_computation.1 | async-start | bytes 1048576 | tf_op jit(solution)/shard_map/all_to_all | solution.py:486
  139.6 17.1 %copy-start.1 = (bf16[16,8,2048]{2,1,0:T(8,128)(2,1)}, bf16[16,8,2048]{2,1,0:T(8,128)(2,1)S(1)}, u32[]{:S(2)}) copy-start(bf16[16,8,2048]{2,1,0:T(8,128)(2,1)S(1)} %all-to-all-done.1) | copy-start | bytes 1572868
  167.8 17.4 %all-to-all-start.2 = ((bf16[16,8,2048]{2,1,0:T(8,128)(2,1)}), bf16[16,8,2048]{2,1,0:T(8,128)(2,1)S(1)}, u32[]{:S(2)}, u32[]{:S(2)}) async-start(bf16[16,8,2048]{2,1,0:T(8,128)(2,1)} %bitcast.27), calls=%async_computation.2 | async-start | bytes 1048576 | tf_op jit(solution)/shard_map/all_to_all | solution.py:489
  185.2 0.8 copy-start.2
Sparse Core Ops, SparseCore 0:
  9.2 147.4 all-gather.2
